TPU v7x, 32 devices: a whole 2x2x4 slice. The times are simulated.
32 devices in a mesh: sp: 4 (over y, x), tp: 8 (over z, core).
Axes of the slice: x: 2, y: 2, z: 4, core: 2. Of those that a mesh axis runs over, the one named last changes fastest.
Arguments:
- tokens: bfloat16 [3, 2048, 4096], P(None, 'sp', 'tp'), may hold values from -6 to 6
- new_token: bfloat16 [3, 1, 4096], P(None, None, 'tp'), may hold values from -6 to 6
- query_weight: bfloat16 [4096, 4096], P(None, 'tp'), may hold values from -0.09375 to 0.09375
- key_weight: bfloat16 [4096, 4096], P(None, 'tp'), may hold values from -0.09375 to 0.09375
- value_weight: bfloat16 [4096, 4096], P(None, 'tp'), may hold values from -0.09375 to 0.09375
- log_decay: float32 [64], P('tp'), may hold values from -0.034 to 0
Outputs:
- state: bfloat16 [3, 64, 64, 64], P(None, 'tp', 'sp')
- read: bfloat16 [3, 4096], P(None, 'tp')
All inputs are finite; a program needn't handle non-finite values.
Results may differ from a plain program's by a relative error of at most 0.012.
Values may be sent and summed in bfloat16 or wider, within the bound.
A program may use at most 64 MiB of HBM per device.

v0:
```python
import functools

import jax
import jax.numpy as jnp
import numpy as np
from jax import lax
from jax.experimental import pallas as pl
from jax.experimental.pallas import tpu as pltpu
from jax.sharding import PartitionSpec as P

HD = 64
LANES = 128
NEW_ROWS = 8
F32 = jnp.float32
BF16 = jnp.bfloat16


def lane_iota(shape):
    return lax.broadcasted_iota(jnp.int32, shape, len(shape) - 1)


def rotated(block, cosine, sine):
    half = HD // 2
    low = lane_iota(block.shape) % HD < half
    swapped = jnp.where(
        low, pltpu.roll(block, LANES - half, 1), pltpu.roll(block, half, 1)
    )
    return block * cosine + swapped * sine


def kernel(
    n_sp, n_tp, parts,
    tokens, fresh, wq_hbm, wk_hbm, wv_hbm, inverse_ref, decay_ref,
    state_out, read_out,
    x, nx, wq, wk, wv, acc_k, acc_v, cos_ref, sin_ref, fade_ref, rows_ref,
    q_spread, own_term, sums, stage, landed, totals,
    load_sem, weight_sem, rx, rn, fwd, share, nfwd, nshare, rs_tx, rs_rx,
):
    seqs, span, feat = tokens.shape
    inner = wk.shape[1]
    heads = inner // HD
    chips = n_tp // 2
    pieces = seqs * parts
    size = span // parts
    keep = HD // n_sp
    sp = lax.axis_index("sp")
    tp = lax.axis_index("tp")
    z, k = tp // 2, tp % 2
    MESH = pl.DeviceIdType.MESH

    def to_tp(index):
        return {"tp": index}

    partner = z * 2 + 1 - k
    own_loads = [
        pltpu.make_async_copy(
            tokens.at[s // parts, pl.ds(s % parts * size, size)], x.at[tp, s], load_sem.at[s]
        )
        for s in range(pieces)
    ]
    new_load = pltpu.make_async_copy(fresh, nx.at[tp], load_sem.at[pieces])
    new_load.start()
    for copy in own_loads:
        copy.start()
    weight_loads = [
        pltpu.make_async_copy(a, b, weight_sem.at[i])
        for i, (a, b) in enumerate(((wk_hbm, wk), (wv_hbm, wv), (wq_hbm, wq)))
    ]

    barrier = pltpu.get_barrier_semaphore()

    @pl.when(z > 0)
    def _():
        pl.semaphore_signal(barrier, inc=1, device_id=to_tp(tp - 2), device_id_type=MESH)

    @pl.when(z < chips - 1)
    def _():
        pl.semaphore_signal(barrier, inc=1, device_id=to_tp(tp + 2), device_id_type=MESH)

    pl.semaphore_signal(barrier, inc=1, device_id=to_tp(partner), device_id_type=MESH)
    for o in range(1, n_sp):
        pl.semaphore_signal(
            barrier, inc=1, device_id={"sp": lax.rem(sp + o, n_sp)}, device_id_type=MESH
        )
    pl.semaphore_wait(
        barrier, n_sp + (z > 0).astype(jnp.int32) + (z < chips - 1).astype(jnp.int32)
    )

    def x_copy(c, s, sem, target):
        p = 2 * c + k
        return pltpu.make_async_remote_copy(
            x.at[p, s], x.at[p, s], sem, rx.at[p, s], device_id=to_tp(target), device_id_type=MESH
        )

    def n_copy(c, sem, target):
        p = 2 * c + k
        return pltpu.make_async_remote_copy(
            nx.at[p], nx.at[p], sem, rn.at[p], device_id=to_tp(target), device_id_type=MESH
        )

    def x_arrived(p, s):
        pltpu.make_async_remote_copy(
            x.at[p, s], x.at[p, s], share.at[0, 0], rx.at[p, s],
            device_id=to_tp(partner), device_id_type=MESH,
        ).wait_recv()

    def n_arrived(p):
        pltpu.make_async_remote_copy(
            nx.at[p], nx.at[p], nshare.at[0], rn.at[p],
            device_id=to_tp(partner), device_id_type=MESH,
        ).wait_recv()

    new_load.wait()
    n_up = n_copy(z, nfwd.at[0, z], tp + 2)
    n_down = n_copy(z, nfwd.at[1, z], tp - 2)
    n_side = n_copy(z, nshare.at[z], partner)

    @pl.when(z < chips - 1)
    def _():
        n_up.start()

    @pl.when(z > 0)
    def _():
        n_down.start()

    n_side.start()
    for s in range(pieces):
        own_loads[s].wait()

        @pl.when(z < chips - 1)
        def _(s=s):
            x_copy(z, s, fwd.at[0, z, s], tp + 2).start()

        @pl.when(z > 0)
        def _(s=s):
            x_copy(z, s, fwd.at[1, z, s], tp - 2).start()

        x_copy(z, s, share.at[z, s], partner).start()

    for copy in weight_loads:
        copy.start()

    row = lax.broadcasted_iota(jnp.int32, (span, LANES), 0)
    within = lane_iota((1, LANES)) % HD
    first_half = jnp.where(within < HD // 2, -1.0, 1.0).astype(F32)
    inverse = inverse_ref[...]
    angles = (sp * span + row).astype(F32) * inverse
    cos_ref[...] = jnp.cos(angles)
    sin_ref[...] = jnp.sin(angles) * first_half
    new_angles = jnp.full((NEW_ROWS, LANES), n_sp * span, F32) * inverse
    new_cos = jnp.cos(new_angles)
    new_sin = jnp.sin(new_angles) * first_half
    head_of = lane_iota((1, inner)) // HD
    rate = jnp.zeros((1, inner), F32)
    for h in range(heads):
        rate = jnp.where(head_of == h, decay_ref[h], rate)
    to_end = (span - 1 - lax.broadcasted_iota(jnp.int32, (span, 1), 0)).astype(F32)
    fade_ref[...] = jnp.exp(to_end * rate)
    rows_ref[0:1] = jnp.exp(rate * (span * (n_sp - 1 - sp)).astype(F32))
    rows_ref[1:2] = jnp.exp(rate)

    for copy in weight_loads:
        copy.wait()

    def add(p, s, fresh_total):
        block = x[p, s]
        where = pl.ds(pl.multiple_of(p * feat, feat), feat)
        part_k = jnp.dot(block, wk[where, :], preferred_element_type=F32)
        part_v = jnp.dot(block, wv[where, :], preferred_element_type=F32)
        if fresh_total:
            acc_k[s] = part_k
            acc_v[s] = part_v
        else:
            acc_k[s] += part_k
            acc_v[s] += part_v

    @pl.loop(0, pieces)
    def _(s):
        add(tp, s, True)
        x_arrived(partner, s)
        add(partner, s, False)

    n_arrived(partner)

    def project_new():
        def piece(p, totals):
            where = pl.ds(pl.multiple_of(p * feat, feat), feat)
            block = jnp.concatenate(
                [nx[p].astype(F32), jnp.zeros((NEW_ROWS - seqs, feat), F32)], axis=0
            ).astype(BF16)
            return tuple(
                t + jnp.dot(block, w[where, :], preferred_element_type=F32)
                for t, w in zip(totals, (wk, wv, wq))
            )

        zero = jnp.zeros((NEW_ROWS, inner), F32)
        new_k, new_v, new_q = lax.fori_loop(0, n_tp, piece, (zero, zero, zero))
        keys, queries = [], []
        for j in range(inner // LANES):
            at = slice(j * LANES, (j + 1) * LANES)
            keys.append((rotated(new_k[:, at], new_cos, new_sin) * HD**-0.5).astype(BF16))
            queries.append(rotated(new_q[:, at], new_cos, new_sin).astype(BF16))
        key = jnp.concatenate(keys, axis=1).astype(F32)
        query = jnp.concatenate(queries, axis=1).astype(F32)
        value = new_v.astype(BF16).astype(F32)
        same = (
            lax.broadcasted_iota(jnp.int32, (inner, inner), 0) // HD
            == lax.broadcasted_iota(jnp.int32, (inner, inner), 1) // HD
        )
        product = query * key
        for h in range(heads):
            at = slice(h * HD, (h + 1) * HD)
            own_term[:, at] = jnp.sum(product[:, at], axis=-1, keepdims=True) * value[:, at]
        pick = lax.broadcasted_iota(jnp.int32, (HD, inner), 0) == lane_iota((HD, inner)) % HD
        for s in range(seqs):
            spread = jnp.where(pick, query[s : s + 1], 0.0).astype(BF16)
            q_spread[s] = jnp.dot(
                spread, jnp.where(same, 1.0, 0.0).astype(BF16), preferred_element_type=F32
            )

    def rs_copy(s, o):
        peer = lax.rem(sp + o, n_sp)
        return pltpu.make_async_remote_copy(
            stage.at[s, peer], landed.at[s, sp], rs_tx.at[s, peer], rs_rx.at[s, sp],
            device_id={"sp": peer}, device_id_type=MESH,
        )

    def finish(i):
        s, part = i // parts, i % parts
        where = pl.ds(pl.multiple_of(part * size, size), size)
        cosine, sine = cos_ref[where, :], sin_ref[where, :]
        lane = lane_iota((HD, LANES))
        for j in range(inner // LANES):
            at = slice(j * LANES, (j + 1) * LANES)
            key = (rotated(acc_k[i, :, at], cosine, sine) * HD**-0.5).astype(BF16)
            weighted = (key.astype(F32) * fade_ref[where, at]).astype(BF16)
            value = acc_v[i, :, at].astype(BF16)
            both = lax.dot_general(
                weighted, value, (((0,), (0,)), ((), ())), preferred_element_type=F32
            )
            state = jnp.where(lane < HD, both[:HD], both[HD:])
            sums[:, at] = jnp.where(part == 0, state, sums[:, at] + state)

        @pl.when(part == parts - 1)
        def _():
            scaled = sums[...] * rows_ref[0:1]
            read = jnp.sum(scaled * q_spread[s], axis=0, keepdims=True)
            for o in range(n_sp):
                stage[s, o, 0:keep] = scaled[o * keep : (o + 1) * keep]
                stage[s, o, keep : keep + 1] = read
            for o in range(1, n_sp):
                rs_copy(s, o).start()
            totals[s] = stage[s, sp]

    far = jnp.maximum(z, chips - 1 - z)

    def decode(i):
        d = i // (2 * pieces) + 1
        s = (i // 2) % pieces
        step = 2 * (i % 2) - 1
        c = z + step * d
        return d, s, step, c, (c >= 0) & (c < chips)

    def onward(step):
        nxt = z - step
        return nxt, (nxt >= 0) & (nxt < chips), (step + 1) // 2

    @pl.loop(0, 2 * pieces * (chips - 1))
    def _(i):
        d, s, step, c, valid = decode(i)
        nxt, pass_on, way = onward(step)

        @pl.when(valid)
        def _():
            @pl.when(s == 0)
            def _():
                n_arrived(2 * c + k)

                @pl.when(pass_on)
                def _():
                    n_copy(c, nfwd.at[way, c], 2 * nxt + k).start()

                n_copy(c, nshare.at[c], partner).start()

            x_arrived(2 * c + k, s)

            @pl.when(pass_on)
            def _():
                x_copy(c, s, fwd.at[way, c, s], 2 * nxt + k).start()

            x_copy(c, s, share.at[c, s], partner).start()
            add(2 * c + k, s, False)

            @pl.when(s == 0)
            def _():
                n_arrived(2 * c + 1 - k)

            x_arrived(2 * c + 1 - k, s)
            add(2 * c + 1 - k, s, False)

        last = (d == far) & (step == 1)

        @pl.when(last & (s == 0))
        def _():
            project_new()

        @pl.when(last)
        def _():
            finish(s)

    raws = []
    for s in range(seqs):
        for o in range(1, n_sp):
            src = lax.rem(sp + o, n_sp)
            pltpu.make_async_remote_copy(
                stage.at[s, src], landed.at[s, src], rs_tx.at[s, src], rs_rx.at[s, src],
                device_id={"sp": src}, device_id_type=MESH,
            ).wait_recv()
        total = None
        for j in range(n_sp):
            term = jnp.where(sp == j, totals[s], landed[s, j])
            total = term if total is None else total + term
        kept = total[0:keep].astype(BF16)
        for h in range(heads):
            state_out[s, h] = kept[:, h * HD : (h + 1) * HD]
        raws.append(total[keep : keep + 1] * rows_ref[1:2] + own_term[s : s + 1])
    raw = jnp.concatenate(raws, axis=0)
    for h in range(heads):
        at = slice(h * HD, (h + 1) * HD)
        head = raw[:, at]
        centered = head - jnp.mean(head, axis=-1, keepdims=True)
        spread = jnp.mean(centered * centered, axis=-1, keepdims=True)
        read_out[:, at] = (centered * lax.rsqrt(spread + 1e-05)).astype(BF16)

    @pl.when(z < chips - 1)
    def _():
        n_up.wait_send()

    @pl.when(z > 0)
    def _():
        n_down.wait_send()

    n_side.wait_send()
    for s in range(seqs):
        for o in range(1, n_sp):
            rs_copy(s, o).wait_send()
    for s in range(pieces):
        @pl.when(z < chips - 1)
        def _(s=s):
            x_copy(z, s, fwd.at[0, z, s], tp + 2).wait_send()

        @pl.when(z > 0)
        def _(s=s):
            x_copy(z, s, fwd.at[1, z, s], tp - 2).wait_send()

        x_copy(z, s, share.at[z, s], partner).wait_send()

    @pl.loop(0, 2 * pieces * (chips - 1))
    def _(i):
        d, s, step, c, valid = decode(i)
        nxt, pass_on, way = onward(step)

        @pl.when(valid)
        def _():
            @pl.when(s == 0)
            def _():
                @pl.when(pass_on)
                def _():
                    n_copy(c, nfwd.at[way, c], 2 * nxt + k).wait_send()

                n_copy(c, nshare.at[c], partner).wait_send()

            @pl.when(pass_on)
            def _():
                x_copy(c, s, fwd.at[way, c, s], 2 * nxt + k).wait_send()

            x_copy(c, s, share.at[c, s], partner).wait_send()


def solution(mesh):
    n_sp, n_tp = mesh.shape["sp"], mesh.shape["tp"]

    def body(tokens, new_token, query_weight, key_weight, value_weight, log_decay):
        seqs, span, feat = tokens.shape
        width, inner = key_weight.shape
        heads = inner // HD
        keep = HD // n_sp
        rows = -(-(keep + 1) // 8) * 8
        chips = n_tp // 2
        half = HD // 2
        parts = max(1, 8 // chips)
        pieces = seqs * parts
        inverse = np.float32(10000.0) ** (-np.arange(half, dtype=np.float32) / half)
        inverse = jnp.asarray(np.tile(inverse.astype(np.float32), LANES // half)[None])
        anywhere = pl.BlockSpec(memory_space=pl.ANY)
        vmem = pl.BlockSpec(memory_space=pltpu.VMEM)
        dma = pltpu.SemaphoreType.DMA
        return pl.pallas_call(
            functools.partial(kernel, n_sp, n_tp, parts),
            out_shape=(
                jax.ShapeDtypeStruct((seqs, heads, keep, HD), BF16),
                jax.ShapeDtypeStruct((seqs, inner), BF16),
            ),
            in_specs=[anywhere] * 5 + [vmem, pl.BlockSpec(memory_space=pltpu.SMEM)],
            out_specs=(vmem, vmem),
            scratch_shapes=[
                pltpu.VMEM((n_tp, pieces, span // parts, feat), BF16),
                pltpu.VMEM((n_tp, seqs, feat), BF16),
                pltpu.VMEM((width, inner), BF16),
                pltpu.VMEM((width, inner), BF16),
                pltpu.VMEM((width, inner), BF16),
                pltpu.VMEM((pieces, span // parts, inner), F32),
                pltpu.VMEM((pieces, span // parts, inner), F32),
                pltpu.VMEM((span, LANES), F32),
                pltpu.VMEM((span, LANES), F32),
                pltpu.VMEM((span, inner), F32),
                pltpu.VMEM((8, inner), F32),
                pltpu.VMEM((seqs, HD, inner), F32),
                pltpu.VMEM((NEW_ROWS, inner), F32),
                pltpu.VMEM((HD, inner), F32),
                pltpu.VMEM((seqs, n_sp, rows, inner), F32),
                pltpu.VMEM((seqs, n_sp, rows, inner), F32),
                pltpu.VMEM((seqs, rows, inner), F32),
                dma((pieces + 1,)),
                dma((3,)),
                dma((n_tp, pieces)),
                dma((n_tp,)),
                dma((2, chips, pieces)),
                dma((chips, pieces)),
                dma((2, chips)),
                dma((chips,)),
                dma((seqs, n_sp)),
                dma((seqs, n_sp)),
            ],
            compiler_params=pltpu.CompilerParams(
                collective_id=0, has_side_effects=True, vmem_limit_bytes=60 * 1024 * 1024
            ),
            name="retention",
        )(tokens, new_token.reshape(seqs, feat), query_weight, key_weight, value_weight, inverse, log_decay)

    return jax.shard_map(
        body,
        mesh=mesh,
        in_specs=(
            P(None, "sp", "tp"),
            P(None, None, "tp"),
            P(None, "tp"),
            P(None, "tp"),
            P(None, "tp"),
            P("tp"),
        ),
        out_specs=(P(None, "tp", "sp", None), P(None, "tp")),
        check_vma=False,
    )
```

profile of v0, /device:TPU:0, one launch (start us, length us, event | category | flops | bytes accessed | tf_op | source)
XLA Modules:
  0.0 120.5 jit_solution(17845041367481463130)
XLA Ops:
  0.6 117.1 %retention.1 = (bf16[3,8,16,64]{3,2,1,0:T(8,128)(2,1)}, bf16[3,512]{1,0:T(4,128)(2,1)}) custom-call(bf16[3,512,512]{2,1,0:T(8,128)(2,1)} %tokens.1, bf16[3,512]{1,0:T(4,128)(2,1)} %bitcast.1, bf16[4096,512]{1,0:T(8,128)(2,1)} %wq_hbm.1, bf16[4096,512]{1,0:T(8,128)(2,1)} %wk_hbm.1, bf16[4096,512]{1,0:T(8,128)(2,1)} %wv_hbm.1, ...), custom_call_target="tpu_custom_call" | custom-call | tf_op jit(solution)/shard_map/retention/pallas_call | solution.py:398
  117.7 1.5 %copy.11 = bf16[3,8,16,64]{3,2,1,0:T(8,128)(2,1)} copy(bf16[3,8,16,64]{3,2,1,0:T(8,128)(2,1)} %get-tuple-element.4) | data formatting | bytes 98304
  119.3 1.3 %copy.12 = bf16[3,512]{1,0:T(4,128)(2,1)} copy(bf16[3,512]{1,0:T(4,128)(2,1)} %get-tuple-element.5) | data formatting | bytes 6144
where the time goes:
time: 121 us
  Pallas kernels  117 us (97%)
  local copies, waits for them, and re-layouts  2.82 us (2%)
    pallas_call x1, Pallas kernels, body(): pl.pallas_call(functools.partial(kernel, n_sp, n_tp, parts), out_shape=(j...  117 us
    unnamed x2, local copies, waits for them, and re-layouts  2.82 us

commit v1 on v0

--- a/solution.py
+++ b/solution.py
@@ -377,6 +377,626 @@
             x_copy(c, s, share.at[c, s], partner).wait_send()
 
 
+def one_of(n, values):
+    total = 0
+    for k, value in enumerate(values):
+        if value:
+            total = total + (n == k).astype(jnp.int32) * value
+    return total
+
+
+def middle_order(main, moved):
+    near = [(0, i) for i in main]
+    far = [(2, i) for i in moved + main]
+    order = [(kind, i) for i in moved for kind in (0, 1)]
+    order += [(1, i) for i in main]
+    for at in range(max(len(near), len(far))):
+        order += near[at : at + 1] + far[at : at + 1]
+    return order
+
+
+def moved_kernel(
+    n_sp, n_tp, parts,
+    tokens, fresh, wq_hbm, wk_hbm, wv_hbm, inverse_ref, decay_ref,
+    state_out, read_out,
+    x, xc, nx, wq, wk, wv, we, acc_k, acc_v, acc_c, cos_ref, sin_ref, fade_ref, rows_ref,
+    q_spread, own_term, sums, stage, landed, totals, hint, hint_in, stage_c, landed_c,
+    load_sem, weight_sem, rx, rn, ry, rw, fwd, share, nsend, ysend, yshare, wsend, wxsend,
+    hint_sem, rs_tx, rs_rx, c_tx, c_rx,
+):
+    seqs, span, feat = tokens.shape
+    inner = wk.shape[1]
+    heads = inner // HD
+    half = inner // 2
+    chunks = half // LANES
+    chips = n_tp // 2
+    pieces = seqs * parts
+    size = span // parts
+    keep = HD // n_sp
+    groups = n_tp // 2
+    moved_seq = seqs - 1
+    main = list(range(moved_seq * parts))
+    moved = list(range(moved_seq * parts, pieces))
+    sp = lax.axis_index("sp")
+    tp = lax.axis_index("tp")
+    z, k = tp // 2, tp % 2
+    row_y, row_x = sp // 2, sp % 2
+    x_peer = sp + 1 - 2 * row_x
+    y_peer = sp + 2 - 4 * row_y
+    MESH = pl.DeviceIdType.MESH
+    end_int = (z == 0).astype(jnp.int32) + (z == chips - 1).astype(jnp.int32)
+    end = end_int > 0
+    mid = end_int == 0
+    partner = z * 2 + 1 - k
+    mate = z + 1 - 2 * (z % 2)
+    mate_tp = 2 * mate + k
+    other = chips - 1 - z
+    other_tp = 2 * other + k
+    second = end_int * (chips - 1 - mate) + (1 - end_int) * (chips - 1 - z)
+    third = end_int * (chips - 1 - z) + (1 - end_int) * (chips - 1 - mate)
+
+    own_loads = {
+        s: pltpu.make_async_copy(
+            tokens.at[s // parts, pl.ds(s % parts * size, size)], x.at[tp, s], load_sem.at[s]
+        )
+        for s in range(pieces)
+    }
+    new_load = pltpu.make_async_copy(fresh, nx.at[tp], load_sem.at[pieces])
+    new_load.start()
+    for s in moved + main:
+        own_loads[s].start()
+    weight_loads = [
+        pltpu.make_async_copy(a, b, weight_sem.at[i])
+        for i, (a, b) in enumerate(((wk_hbm, wk), (wv_hbm, wv), (wq_hbm, wq)))
+    ]
+
+    barrier = pltpu.get_barrier_semaphore()
+    for o in range(1, n_tp):
+        pl.semaphore_signal(
+            barrier, inc=1, device_id={"tp": lax.rem(tp + o, n_tp)}, device_id_type=MESH
+        )
+    for o in range(1, n_sp):
+        pl.semaphore_signal(
+            barrier, inc=1, device_id={"sp": lax.rem(sp + o, n_sp)}, device_id_type=MESH
+        )
+        pl.semaphore_signal(
+            barrier, inc=1, device_id={"sp": lax.rem(sp + o, n_sp), "tp": mate_tp},
+            device_id_type=MESH,
+        )
+    pl.semaphore_wait(barrier, n_tp - 1 + 2 * (n_sp - 1))
+
+    def x_copy(c, s, sem, target):
+        p = 2 * c + k
+        return pltpu.make_async_remote_copy(
+            x.at[p, s], x.at[p, s], sem, rx.at[p, s],
+            device_id={"tp": target}, device_id_type=MESH,
+        )
+
+    def to_mate(c, s):
+        return x_copy(c, s, fwd.at[0, c, s], mate_tp)
+
+    def to_other(c, s):
+        return x_copy(c, s, fwd.at[1, c, s], other_tp)
+
+    def to_partner(c, s):
+        return x_copy(c, s, share.at[c, s], partner)
+
+    def x_arrived(p, s):
+        pltpu.make_async_remote_copy(
+            x.at[p, s], x.at[p, s], share.at[0, 0], rx.at[p, s],
+            device_id={"tp": partner}, device_id_type=MESH,
+        ).wait_recv()
+
+    def y_send(c, j):
+        p = 2 * c + k
+        return pltpu.make_async_remote_copy(
+            x.at[p, moved[0] + j], xc.at[p, j], ysend.at[c, j], ry.at[p, j],
+            device_id={"sp": y_peer}, device_id_type=MESH,
+        )
+
+    def y_share(c, j):
+        p = 2 * c + k
+        return pltpu.make_async_remote_copy(
+            xc.at[p, j], xc.at[p, j], yshare.at[c, j], ry.at[p, j],
+            device_id={"tp": partner}, device_id_type=MESH,
+        )
+
+    def y_arrived(p, j):
+        pltpu.make_async_remote_copy(
+            xc.at[p, j], xc.at[p, j], yshare.at[0, 0], ry.at[p, j],
+            device_id={"tp": partner}, device_id_type=MESH,
+        ).wait_recv()
+
+    def w_rows(p):
+        return pl.ds(pl.multiple_of(p * feat, feat), feat)
+
+    def w_cols(cc):
+        return pl.ds(pl.multiple_of(row_y * half + cc * LANES, LANES), LANES)
+
+    def w_send(cc, g, kv):
+        p = row_x * groups + g
+        return pltpu.make_async_remote_copy(
+            (wk, wv)[kv].at[w_rows(p), w_cols(cc)],
+            we.at[cc, w_rows(p), pl.ds(kv * LANES, LANES)],
+            wsend.at[cc, g, kv], rw.at[cc, p, kv],
+            device_id={"tp": mate_tp}, device_id_type=MESH,
+        )
+
+    def w_pass(cc, g, kv):
+        p = row_x * groups + g
+        where = we.at[cc, w_rows(p), pl.ds(kv * LANES, LANES)]
+        return pltpu.make_async_remote_copy(
+            where, where, wxsend.at[cc, g, kv], rw.at[cc, p, kv],
+            device_id={"sp": x_peer}, device_id_type=MESH,
+        )
+
+    def w_arrived(cc, p, kv):
+        where = we.at[cc, w_rows(p), pl.ds(kv * LANES, LANES)]
+        pltpu.make_async_remote_copy(
+            where, where, wxsend.at[cc, 0, kv], rw.at[cc, p, kv],
+            device_id={"sp": x_peer}, device_id_type=MESH,
+        ).wait_recv()
+
+    def n_copy(o):
+        return pltpu.make_async_remote_copy(
+            nx.at[tp], nx.at[tp], nsend.at[o], rn.at[tp],
+            device_id={"tp": lax.rem(tp + o, n_tp)}, device_id_type=MESH,
+        )
+
+    def n_arrived(o):
+        p = lax.rem(tp + o, n_tp)
+        pltpu.make_async_remote_copy(
+            nx.at[p], nx.at[p], nsend.at[0], rn.at[p],
+            device_id={"tp": p}, device_id_type=MESH,
+        ).wait_recv()
+
+    hint_copy = pltpu.make_async_remote_copy(
+        hint, hint_in, hint_sem.at[0], hint_sem.at[1],
+        device_id={"tp": mate_tp}, device_id_type=MESH,
+    )
+
+    new_load.wait()
+    for o in range(1, n_tp):
+        n_copy(o).start()
+    for j, s in enumerate(moved):
+        own_loads[s].wait()
+
+        @pl.when(mid)
+        def _(j=j, s=s):
+            to_other(z, s).start()
+            y_send(z, j).start()
+            to_partner(z, s).start()
+
+        @pl.when(end)
+        def _(s=s):
+            to_mate(z, s).start()
+
+    for s in main:
+        own_loads[s].wait()
+        to_partner(z, s).start()
+
+        @pl.when(mid)
+        def _(s=s):
+            to_mate(z, s).start()
+            to_other(z, s).start()
+
+    for copy in weight_loads:
+        copy.start()
+
+    row = lax.broadcasted_iota(jnp.int32, (span, LANES), 0)
+    within = lane_iota((1, LANES)) % HD
+    first_half = jnp.where(within < HD // 2, -1.0, 1.0).astype(F32)
+    inverse = inverse_ref[...]
+
+    def tables(slot, column):
+        angles = (column * span + row).astype(F32) * inverse
+        cos_ref[slot] = jnp.cos(angles)
+        sin_ref[slot] = jnp.sin(angles) * first_half
+
+    for copy in weight_loads[:2]:
+        copy.wait()
+
+    @pl.when(end)
+    def _():
+        for g in range(groups):
+            for kv in range(2):
+                w_send(0, g, kv).start()
+        for s in main:
+            to_mate(z, s).start()
+        for cc in range(1, chunks):
+            for g in range(groups):
+                for kv in range(2):
+                    w_send(cc, g, kv).start()
+
+    tables(0, sp)
+
+    @pl.when(mid)
+    def _():
+        tables(1, y_peer)
+
+    new_angles = jnp.full((NEW_ROWS, LANES), n_sp * span, F32) * inverse
+    new_cos = jnp.cos(new_angles)
+    new_sin = jnp.sin(new_angles) * first_half
+    head_of = lane_iota((1, inner)) // HD
+    rate = jnp.zeros((1, inner), F32)
+    for h in range(heads):
+        rate = jnp.where(head_of == h, decay_ref[h], rate)
+    to_end = (span - 1 - lax.broadcasted_iota(jnp.int32, (span, 1), 0)).astype(F32)
+    fade_ref[...] = jnp.exp(to_end * rate)
+    rows_ref[0:1] = jnp.exp(rate * (span * (n_sp - 1 - sp)).astype(F32))
+    rows_ref[1:2] = jnp.exp(rate)
+    hint[...] = jnp.zeros(hint.shape, F32)
+    hint[1:2] = rate
+    weight_loads[2].wait()
+
+    def add(p, s, fresh_total):
+        block = x[p, s]
+        where = w_rows(p)
+        part_k = jnp.dot(block, wk[where, :], preferred_element_type=F32)
+        part_v = jnp.dot(block, wv[where, :], preferred_element_type=F32)
+        if fresh_total:
+            acc_k[s] = part_k
+            acc_v[s] = part_v
+        else:
+            acc_k[s] += part_k
+            acc_v[s] += part_v
+
+    own_pieces = end_int * len(main) + (1 - end_int) * pieces
+
+    @pl.loop(0, pieces)
+    def _(i):
+        s = lax.rem(i + (1 - end_int) * len(main), pieces)
+
+        @pl.when(i < own_pieces)
+        def _():
+            add(tp, s, True)
+
+        @pl.when(i < own_pieces)
+        def _():
+            x_arrived(partner, s)
+            add(partner, s, False)
+
+    for o in range(1, n_tp):
+        n_arrived(o)
+
+    same = (
+        lax.broadcasted_iota(jnp.int32, (inner, inner), 0) // HD
+        == lax.broadcasted_iota(jnp.int32, (inner, inner), 1) // HD
+    )
+    pick = lax.broadcasted_iota(jnp.int32, (HD, inner), 0) == lane_iota((HD, inner)) % HD
+
+    def project_new():
+        def piece(p, totals):
+            where = w_rows(p)
+            block = jnp.concatenate(
+                [nx[p].astype(F32), jnp.zeros((NEW_ROWS - seqs, feat), F32)], axis=0
+            ).astype(BF16)
+            return tuple(
+                t + jnp.dot(block, w[where, :], preferred_element_type=F32)
+                for t, w in zip(totals, (wk, wv, wq))
+            )
+
+        zero = jnp.zeros((NEW_ROWS, inner), F32)
+        new_k, new_v, new_q = lax.fori_loop(0, n_tp, piece, (zero, zero, zero))
+        keys, queries = [], []
+        for j in range(inner // LANES):
+            at = slice(j * LANES, (j + 1) * LANES)
+            keys.append((rotated(new_k[:, at], new_cos, new_sin) * HD**-0.5).astype(BF16))
+            queries.append(rotated(new_q[:, at], new_cos, new_sin).astype(BF16))
+        key = jnp.concatenate(keys, axis=1).astype(F32)
+        query = jnp.concatenate(queries, axis=1).astype(F32)
+        value = new_v.astype(BF16).astype(F32)
+        product = query * key
+        for h in range(heads):
+            at = slice(h * HD, (h + 1) * HD)
+            own_term[:, at] = jnp.sum(product[:, at], axis=-1, keepdims=True) * value[:, at]
+        hint[0:1] = query[moved_seq : moved_seq + 1]
+        for s in range(seqs):
+            spread = jnp.where(pick, query[s : s + 1], 0.0).astype(BF16)
+            q_spread[s] = jnp.dot(
+                spread, jnp.where(same, 1.0, 0.0).astype(BF16), preferred_element_type=F32
+            )
+
+    project_new()
+
+    @pl.when(end)
+    def _():
+        hint_copy.start()
+
+    def rs_copy(s, o):
+        peer = lax.rem(sp + o, n_sp)
+        return pltpu.make_async_remote_copy(
+            stage.at[s, peer], landed.at[s, sp], rs_tx.at[s, peer], rs_rx.at[s, sp],
+            device_id={"sp": peer}, device_id_type=MESH,
+        )
+
+    def outer(weighted, value):
+        both = lax.dot_general(
+            weighted, value, (((0,), (0,)), ((), ())), preferred_element_type=F32
+        )
+        return jnp.where(lane_iota((HD, LANES)) < HD, both[:HD], both[HD:])
+
+    def finish(i):
+        s, part = i // parts, i % parts
+        where = pl.ds(pl.multiple_of(part * size, size), size)
+        cosine, sine = cos_ref[0, where, :], sin_ref[0, where, :]
+        for j in range(inner // LANES):
+            at = slice(j * LANES, (j + 1) * LANES)
+            key = (rotated(acc_k[i, :, at], cosine, sine) * HD**-0.5).astype(BF16)
+            weighted = (key.astype(F32) * fade_ref[where, at]).astype(BF16)
+            value = acc_v[i, :, at].astype(BF16)
+            state = outer(weighted, value)
+            sums[:, at] = jnp.where(part == 0, state, sums[:, at] + state)
+
+        @pl.when(part == parts - 1)
+        def _():
+            scaled = sums[...] * rows_ref[0:1]
+            read = jnp.sum(scaled * q_spread[s], axis=0, keepdims=True)
+            for o in range(n_sp):
+                stage[s, o, 0:keep] = scaled[o * keep : (o + 1) * keep]
+                stage[s, o, keep : keep + 1] = read
+            for o in range(1, n_sp):
+                rs_copy(s, o).start()
+            totals[s] = stage[s, sp]
+
+    def c_add(cc, p, fresh_total):
+        where = w_rows(p)
+        for t in range(parts):
+            for side, block in ((0, x[p, moved[0] + t]), (1, xc[p, t])):
+                both = jnp.dot(block, we[cc, where, :], preferred_element_type=F32)
+                if fresh_total:
+                    acc_c[side, t] = both
+                else:
+                    acc_c[side, t] += both
+
+    def c_copy(cc, o):
+        return pltpu.make_async_remote_copy(
+            stage_c.at[cc, o], landed_c.at[cc, sp], c_tx.at[cc, o], c_rx.at[cc, sp],
+            device_id={"sp": o, "tp": mate_tp}, device_id_type=MESH,
+        )
+
+    def c_finish(cc):
+        pair_rate = hint_in[1:2, w_cols(cc)]
+        query = hint_in[0:1, w_cols(cc)]
+        total = jnp.zeros((HD, LANES), F32)
+        for side, column in ((0, sp), (1, y_peer)):
+            state = jnp.zeros((HD, LANES), F32)
+            for t in range(parts):
+                at = slice(t * size, (t + 1) * size)
+                key = (
+                    rotated(acc_c[side, t, :, :LANES], cos_ref[side, at], sin_ref[side, at])
+                    * HD**-0.5
+                ).astype(BF16)
+                fade = jnp.exp(to_end[at] * pair_rate)
+                weighted = (key.astype(F32) * fade).astype(BF16)
+                state = state + outer(weighted, acc_c[side, t, :, LANES:].astype(BF16))
+            total = total + state * jnp.exp(
+                pair_rate * (span * (n_sp - 1 - column)).astype(F32)
+            )
+        spread = jnp.where(pick[:, :LANES], query, 0.0).astype(BF16)
+        spread = jnp.dot(
+            spread, jnp.where(same[:LANES, :LANES], 1.0, 0.0).astype(BF16),
+            preferred_element_type=F32,
+        )
+        read = jnp.sum(total * spread, axis=0, keepdims=True)
+        for o in range(n_sp):
+            stage_c[cc, o, 0:keep] = total[o * keep : (o + 1) * keep]
+            stage_c[cc, o, keep : keep + 1] = read
+        for o in range(n_sp):
+            c_copy(cc, o).start()
+
+    order = middle_order(main, moved)
+    steps = end_int * (len(main) * (chips - 1)) + (1 - end_int) * len(order)
+
+    def decode(n):
+        kind = end_int * (n // len(main)) + (1 - end_int) * one_of(n, [o[0] for o in order])
+        s = end_int * (n % len(main)) + (1 - end_int) * one_of(n, [o[1] for o in order])
+        c = (
+            (kind == 0).astype(jnp.int32) * mate
+            + (kind == 1).astype(jnp.int32) * second
+            + (kind == 2).astype(jnp.int32) * third
+        )
+        return kind, c, s
+
+    first_w = 2 * len(moved) + 1
+    c_at = len(order) - 2
+
+    def y_pass(c, j):
+        y_arrived(2 * c + k, j)
+        y_share(c, j).start()
+
+    @pl.loop(0, len(order) + 1)
+    def _(n):
+        kind, c, s = decode(n)
+        is_moved = s >= moved[0]
+
+        @pl.when(n < steps)
+        def _():
+            x_arrived(2 * c + k, s)
+
+            @pl.when(mid & (kind == 0))
+            def _():
+                to_other(c, s).start()
+
+            @pl.when(mid & (kind > 0) & (s < moved[0]))
+            def _():
+                to_mate(c, s).start()
+
+            @pl.when(mid & is_moved)
+            def _():
+                y_send(c, s - moved[0]).start()
+
+            to_partner(c, s).start()
+
+        @pl.when(mid & (n >= first_w) & (n < first_w + groups))
+        def _():
+            for kv in range(2):
+                w_arrived(0, row_x * groups + n - first_w, kv)
+                w_pass(0, n - first_w, kv).start()
+
+        @pl.when(mid & (n >= 3) & (n < 3 + parts))
+        def _():
+            y_pass(z, n - 3)
+
+        @pl.when(mid & (n >= 6) & (n < 6 + 2 * parts))
+        def _():
+            m = n - 6
+            y_pass((m % 2) * second + (1 - m % 2) * mate, m // 2)
+
+        @pl.when(mid & (n >= c_at - parts) & (n < c_at))
+        def _():
+            y_pass(third, n - (c_at - parts))
+
+        @pl.when(n < steps)
+        def _():
+            add(2 * c + k, s, False)
+
+        kind_b, c_b, s_b = decode(n - 1)
+
+        @pl.when((n >= 1) & (n <= steps))
+        def _():
+            x_arrived(2 * c_b + 1 - k, s_b)
+            add(2 * c_b + 1 - k, s_b, False)
+
+            @pl.when(kind_b == 2)
+            def _():
+                finish(s_b)
+
+        @pl.when(mid & (n == c_at))
+        def _():
+            for cx in range(chips):
+                for j in range(parts):
+                    y_arrived(2 * cx + 1 - k, j)
+            for g in range(groups):
+                for kv in range(2):
+                    w_arrived(0, (1 - row_x) * groups + g, kv)
+            c_add(0, 0, True)
+
+            @pl.loop(1, n_tp)
+            def _(p):
+                c_add(0, p, False)
+
+            hint_copy.wait_recv()
+            c_finish(0)
+
+    @pl.when(mid)
+    def _():
+        for cc in range(1, chunks):
+            for g in range(groups + 1):
+                if g < groups:
+                    for kv in range(2):
+                        w_arrived(cc, row_x * groups + g, kv)
+                        w_pass(cc, g, kv).start()
+                    c_add(cc, row_x * groups + g, g == 0)
+                if g > 0:
+                    for kv in range(2):
+                        w_arrived(cc, (1 - row_x) * groups + g - 1, kv)
+                    c_add(cc, (1 - row_x) * groups + g - 1, False)
+            c_finish(cc)
+
+    def gather(s):
+        for o in range(1, n_sp):
+            src = lax.rem(sp + o, n_sp)
+            pltpu.make_async_remote_copy(
+                stage.at[s, src], landed.at[s, src], rs_tx.at[s, src], rs_rx.at[s, src],
+                device_id={"sp": src}, device_id_type=MESH,
+            ).wait_recv()
+        total = None
+        for j in range(n_sp):
+            term = jnp.where(sp == j, totals[s], landed[s, j])
+            total = term if total is None else total + term
+        totals[s] = total
+
+    for s in range(moved_seq):
+        gather(s)
+
+    @pl.when(mid)
+    def _():
+        gather(moved_seq)
+
+    @pl.when(end)
+    def _():
+        for cc in range(chunks):
+            for o in range(n_sp):
+                pltpu.make_async_remote_copy(
+                    stage_c.at[cc, o], landed_c.at[cc, o], c_tx.at[cc, o], c_rx.at[cc, o],
+                    device_id={"sp": o, "tp": mate_tp}, device_id_type=MESH,
+                ).wait_recv()
+            for side in range(2):
+                at = slice(side * half + cc * LANES, side * half + (cc + 1) * LANES)
+                totals[moved_seq, :, at] = landed_c[cc, 2 * side] + landed_c[cc, 2 * side + 1]
+
+    raws = []
+    for s in range(seqs):
+        total = totals[s]
+        kept = total[0:keep].astype(BF16)
+        for h in range(heads):
+            state_out[s, h] = kept[:, h * HD : (h + 1) * HD]
+        raws.append(total[keep : keep + 1] * rows_ref[1:2] + own_term[s : s + 1])
+    raw = jnp.concatenate(raws, axis=0)
+    for h in range(heads):
+        at = slice(h * HD, (h + 1) * HD)
+        head = raw[:, at]
+        centered = head - jnp.mean(head, axis=-1, keepdims=True)
+        spread = jnp.mean(centered * centered, axis=-1, keepdims=True)
+        read_out[:, at] = (centered * lax.rsqrt(spread + 1e-05)).astype(BF16)
+
+    for o in range(1, n_tp):
+        n_copy(o).wait_send()
+    for s in main:
+        to_partner(z, s).wait_send()
+        to_mate(z, s).wait_send()
+        for o in range(1, n_sp):
+            if s % parts == 0:
+                rs_copy(s // parts, o).wait_send()
+
+    @pl.when(end)
+    def _():
+        hint_copy.wait_send()
+        for s in moved:
+            to_mate(z, s).wait_send()
+        for cc in range(chunks):
+            for g in range(groups):
+                for kv in range(2):
+                    w_send(cc, g, kv).wait_send()
+
+    @pl.when(mid)
+    def _():
+        for j, s in enumerate(moved):
+            to_other(z, s).wait_send()
+            to_partner(z, s).wait_send()
+        for s in main:
+            to_other(z, s).wait_send()
+        for cx in range(chips):
+            for j in range(parts):
+                y_send(cx, j).wait_send()
+                y_share(cx, j).wait_send()
+        for o in range(1, n_sp):
+            rs_copy(moved_seq, o).wait_send()
+        for cc in range(chunks):
+            for g in range(groups):
+                for kv in range(2):
+                    w_pass(cc, g, kv).wait_send()
+            for o in range(n_sp):
+                c_copy(cc, o).wait_send()
+
+    @pl.loop(0, len(order))
+    def _(n):
+        kind, c, s = decode(n)
+
+        @pl.when(n < steps)
+        def _():
+            @pl.when(mid & (kind == 0))
+            def _():
+                to_other(c, s).wait_send()
+
+            @pl.when(mid & (kind > 0) & (s < moved[0]))
+            def _():
+                to_mate(c, s).wait_send()
+
+            to_partner(c, s).wait_send()
+
+
 def solution(mesh):
     n_sp, n_tp = mesh.shape["sp"], mesh.shape["tp"]
 
@@ -390,48 +1010,105 @@
         half = HD // 2
         parts = max(1, 8 // chips)
         pieces = seqs * parts
+        size = span // parts
         inverse = np.float32(10000.0) ** (-np.arange(half, dtype=np.float32) / half)
         inverse = jnp.asarray(np.tile(inverse.astype(np.float32), LANES // half)[None])
         anywhere = pl.BlockSpec(memory_space=pl.ANY)
         vmem = pl.BlockSpec(memory_space=pltpu.VMEM)
         dma = pltpu.SemaphoreType.DMA
+        moves = chips == 4 and n_sp == 4 and seqs > 1 and inner % (2 * LANES) == 0
+        tokens_in = [
+            pltpu.VMEM((n_tp, pieces, size, feat), BF16),
+            pltpu.VMEM((n_tp, seqs, feat), BF16),
+        ]
+        weights_in = [pltpu.VMEM((width, inner), BF16)] * 3
+        totals = [pltpu.VMEM((pieces, size, inner), F32)] * 2
+        ends = [
+            pltpu.VMEM((8, inner), F32),
+            pltpu.VMEM((seqs, HD, inner), F32),
+            pltpu.VMEM((NEW_ROWS, inner), F32),
+            pltpu.VMEM((HD, inner), F32),
+            pltpu.VMEM((seqs, n_sp, rows, inner), F32),
+            pltpu.VMEM((seqs, n_sp, rows, inner), F32),
+            pltpu.VMEM((seqs, rows, inner), F32),
+        ]
+        if moves:
+            chunks = inner // 2 // LANES
+            groups = n_tp // 2
+            call = moved_kernel
+            scratch = (
+                tokens_in[:1]
+                + [pltpu.VMEM((n_tp, parts, size, feat), BF16)]
+                + tokens_in[1:]
+                + weights_in
+                + [pltpu.VMEM((chunks, width, 2 * LANES), BF16)]
+                + totals
+                + [
+                    pltpu.VMEM((2, parts, size, 2 * LANES), F32),
+                    pltpu.VMEM((2, span, LANES), F32),
+                    pltpu.VMEM((2, span, LANES), F32),
+                    pltpu.VMEM((span, inner), F32),
+                ]
+                + ends
+                + [
+                    pltpu.VMEM((8, inner), F32),
+                    pltpu.VMEM((8, inner), F32),
+                    pltpu.VMEM((chunks, n_sp, rows, LANES), F32),
+                    pltpu.VMEM((chunks, n_sp, rows, LANES), F32),
+                    dma((pieces + 1,)),
+                    dma((3,)),
+                    dma((n_tp, pieces)),
+                    dma((n_tp,)),
+                    dma((n_tp, parts)),
+                    dma((chunks, n_tp, 2)),
+                    dma((2, chips, pieces)),
+                    dma((chips, pieces)),
+                    dma((n_tp,)),
+                    dma((chips, parts)),
+                    dma((chips, parts)),
+                    dma((chunks, groups, 2)),
+                    dma((chunks, groups, 2)),
+                    dma((2,)),
+                    dma((seqs, n_sp)),
+                    dma((seqs, n_sp)),
+                    dma((chunks, n_sp)),
+                    dma((chunks, n_sp)),
+                ]
+            )
+        else:
+            call = kernel
+            scratch = (
+                tokens_in
+                + weights_in
+                + totals
+                + [
+                    pltpu.VMEM((span, LANES), F32),
+                    pltpu.VMEM((span, LANES), F32),
+                    pltpu.VMEM((span, inner), F32),
+                ]
+                + ends
+                + [
+                    dma((pieces + 1,)),
+                    dma((3,)),
+                    dma((n_tp, pieces)),
+                    dma((n_tp,)),
+                    dma((2, chips, pieces)),
+                    dma((chips, pieces)),
+                    dma((2, chips)),
+                    dma((chips,)),
+                    dma((seqs, n_sp)),
+                    dma((seqs, n_sp)),
+                ]
+            )
         return pl.pallas_call(
-            functools.partial(kernel, n_sp, n_tp, parts),
+            functools.partial(call, n_sp, n_tp, parts),
             out_shape=(
                 jax.ShapeDtypeStruct((seqs, heads, keep, HD), BF16),
                 jax.ShapeDtypeStruct((seqs, inner), BF16),
             ),
             in_specs=[anywhere] * 5 + [vmem, pl.BlockSpec(memory_space=pltpu.SMEM)],
             out_specs=(vmem, vmem),
-            scratch_shapes=[
-                pltpu.VMEM((n_tp, pieces, span // parts, feat), BF16),
-                pltpu.VMEM((n_tp, seqs, feat), BF16),
-                pltpu.VMEM((width, inner), BF16),
-                pltpu.VMEM((width, inner), BF16),
-                pltpu.VMEM((width, inner), BF16),
-                pltpu.VMEM((pieces, span // parts, inner), F32),
-                pltpu.VMEM((pieces, span // parts, inner), F32),
-                pltpu.VMEM((span, LANES), F32),
-                pltpu.VMEM((span, LANES), F32),
-                pltpu.VMEM((span, inner), F32),
-                pltpu.VMEM((8, inner), F32),
-                pltpu.VMEM((seqs, HD, inner), F32),
-                pltpu.VMEM((NEW_ROWS, inner), F32),
-                pltpu.VMEM((HD, inner), F32),
-                pltpu.VMEM((seqs, n_sp, rows, inner), F32),
-                pltpu.VMEM((seqs, n_sp, rows, inner), F32),
-                pltpu.VMEM((seqs, rows, inner), F32),
-                dma((pieces + 1,)),
-                dma((3,)),
-                dma((n_tp, pieces)),
-                dma((n_tp,)),
-                dma((2, chips, pieces)),
-                dma((chips, pieces)),
-                dma((2, chips)),
-                dma((chips,)),
-                dma((seqs, n_sp)),
-                dma((seqs, n_sp)),
-            ],
+            scratch_shapes=scratch,
             compiler_params=pltpu.CompilerParams(
                 collective_id=0, has_side_effects=True, vmem_limit_bytes=60 * 1024 * 1024
             ),

time: 121 us -> 131 us (1.083)
  Pallas kernels: 117 us -> 127 us
    pallas_call x1, Pallas kernels: 117 us -> 127 us  [body(): pl.pallas_call(functools.partial(call, n_sp, n_tp, parts), out_shape=(jax...]
where the time goes in v1:
time: 131 us; the launch traced here: 130 us
  Pallas kernels  127 us (97%)
  local copies, waits for them, and re-layouts  2.82 us (2%)
    pallas_call x1, Pallas kernels, body(): pl.pallas_call(functools.partial(call, n_sp, n_tp, parts), out_shape=(jax...  127 us
    unnamed x2, local copies, waits for them, and re-layouts  2.82 us

profile of v1, /device:TPU:0, one launch (start us, length us, event | category | flops | bytes accessed | tf_op | source)
XLA Modules:
  0.0 130.4 jit_solution(2436435233018377783)
XLA Ops:
  0.6 127.0 %retention.1 = (bf16[3,8,16,64]{3,2,1,0:T(8,128)(2,1)}, bf16[3,512]{1,0:T(4,128)(2,1)}) custom-call(bf16[3,512,512]{2,1,0:T(8,128)(2,1)} %tokens.1, bf16[3,512]{1,0:T(4,128)(2,1)} %bitcast.1, bf16[4096,512]{1,0:T(8,128)(2,1)} %wq_hbm.1, bf16[4096,512]{1,0:T(8,128)(2,1)} %wk_hbm.1, bf16[4096,512]{1,0:T(8,128)(2,1)} %wv_hbm.1, ...), custom_call_target="tpu_custom_call" | custom-call | tf_op jit(solution)/shard_map/retention/pallas_call | solution.py:1103
  127.6 1.5 %copy.11 = bf16[3,8,16,64]{3,2,1,0:T(8,128)(2,1)} copy(bf16[3,8,16,64]{3,2,1,0:T(8,128)(2,1)} %get-tuple-element.4) | data formatting | bytes 98304
  129.1 1.3 copy.12

commit v2 on v1

--- a/solution.py
+++ b/solution.py
@@ -601,12 +601,6 @@
         for g in range(groups):
             for kv in range(2):
                 w_send(0, g, kv).start()
-        for s in main:
-            to_mate(z, s).start()
-        for cc in range(1, chunks):
-            for g in range(groups):
-                for kv in range(2):
-                    w_send(cc, g, kv).start()
 
     tables(0, sp)
 
@@ -641,29 +635,28 @@
             acc_k[s] += part_k
             acc_v[s] += part_v
 
-    own_pieces = end_int * len(main) + (1 - end_int) * pieces
-
-    @pl.loop(0, pieces)
-    def _(i):
-        s = lax.rem(i + (1 - end_int) * len(main), pieces)
-
-        @pl.when(i < own_pieces)
-        def _():
-            add(tp, s, True)
-
-        @pl.when(i < own_pieces)
-        def _():
-            x_arrived(partner, s)
-            add(partner, s, False)
-
-    for o in range(1, n_tp):
-        n_arrived(o)
-
     same = (
         lax.broadcasted_iota(jnp.int32, (inner, inner), 0) // HD
         == lax.broadcasted_iota(jnp.int32, (inner, inner), 1) // HD
     )
     pick = lax.broadcasted_iota(jnp.int32, (HD, inner), 0) == lane_iota((HD, inner)) % HD
+    own_pieces = end_int * len(main) + (1 - end_int) * pieces
+
+    @pl.loop(0, pieces)
+    def _(i):
+        s = lax.rem(i + (1 - end_int) * len(main), pieces)
+
+        @pl.when(i < own_pieces)
+        def _():
+            add(tp, s, True)
+
+        @pl.when(i < own_pieces)
+        def _():
+            x_arrived(partner, s)
+            add(partner, s, False)
+
+    for o in range(1, n_tp):
+        n_arrived(o)
 
     def project_new():
         def piece(p, totals):
@@ -702,6 +695,12 @@
     @pl.when(end)
     def _():
         hint_copy.start()
+        for s in main:
+            to_mate(z, s).start()
+        for cc in range(1, chunks):
+            for g in range(groups):
+                for kv in range(2):
+                    w_send(cc, g, kv).start()
 
     def rs_copy(s, o):
         peer = lax.rem(sp + o, n_sp)
@@ -735,9 +734,12 @@
             for o in range(n_sp):
                 stage[s, o, 0:keep] = scaled[o * keep : (o + 1) * keep]
                 stage[s, o, keep : keep + 1] = read
-            for o in range(1, n_sp):
-                rs_copy(s, o).start()
             totals[s] = stage[s, sp]
+
+            @pl.when(end | (s == moved_seq))
+            def _():
+                for o in range(1, n_sp):
+                    rs_copy(s, o).start()
 
     def c_add(cc, p, fresh_total):
         where = w_rows(p)
@@ -799,7 +801,19 @@
         return kind, c, s
 
     first_w = 2 * len(moved) + 1
-    c_at = len(order) - 2
+    c_at = len(order) - 3
+
+    def w_relay(cc, g, kv):
+        w_arrived(cc, row_x * groups + g, kv)
+        w_pass(cc, g, kv).start()
+
+    def w_own(cc, g, fresh_total=False):
+        c_add(cc, row_x * groups + g, fresh_total)
+
+    def w_peer(cc, g):
+        for kv in range(2):
+            w_arrived(cc, (1 - row_x) * groups + g, kv)
+        c_add(cc, (1 - row_x) * groups + g, False)
 
     def y_pass(c, j):
         y_arrived(2 * c + k, j)
@@ -810,6 +824,14 @@
         kind, c, s = decode(n)
         is_moved = s >= moved[0]
 
+        @pl.when(mid & (n == len(order) - 2))
+        def _():
+            w_relay(1, 0, 1)
+
+        @pl.when(mid & (n == len(order) - 1))
+        def _():
+            w_relay(1, 1, 0)
+
         @pl.when(n < steps)
         def _():
             x_arrived(2 * c + k, s)
@@ -828,11 +850,14 @@
 
             to_partner(c, s).start()
 
+        @pl.when(mid & (n == len(order) - 1))
+        def _():
+            w_relay(1, 1, 1)
+
         @pl.when(mid & (n >= first_w) & (n < first_w + groups))
         def _():
             for kv in range(2):
-                w_arrived(0, row_x * groups + n - first_w, kv)
-                w_pass(0, n - first_w, kv).start()
+                w_relay(0, n - first_w, kv)
 
         @pl.when(mid & (n >= 3) & (n < 3 + parts))
         def _():
@@ -862,37 +887,60 @@
             def _():
                 finish(s_b)
 
-        @pl.when(mid & (n == c_at))
-        def _():
-            for cx in range(chips):
+        early = n - (c_at - 5)
+
+        @pl.when(mid & (early == 0))
+        def _():
+            for cx in (z, mate, second):
                 for j in range(parts):
                     y_arrived(2 * cx + 1 - k, j)
             for g in range(groups):
                 for kv in range(2):
                     w_arrived(0, (1 - row_x) * groups + g, kv)
-            c_add(0, 0, True)
-
-            @pl.loop(1, n_tp)
-            def _(p):
-                c_add(0, p, False)
+            acc_c[...] = jnp.zeros(acc_c.shape, F32)
+
+        @pl.when(mid & (early >= 0) & (early < 6))
+        def _():
+            turn = early // 2
+            cx = (
+                (turn == 0).astype(jnp.int32) * z
+                + (turn == 1).astype(jnp.int32) * mate
+                + (turn == 2).astype(jnp.int32) * second
+            )
+            c_add(0, 2 * cx + early % 2, False)
+
+        @pl.when(mid & (n == c_at))
+        def _():
+            for j in range(parts):
+                y_arrived(2 * third + 1 - k, j)
+
+            @pl.loop(0, 2)
+            def _(m):
+                c_add(0, 2 * third + m, False)
+
+            w_relay(1, 0, 0)
 
             hint_copy.wait_recv()
             c_finish(0)
 
     @pl.when(mid)
     def _():
-        for cc in range(1, chunks):
-            for g in range(groups + 1):
-                if g < groups:
-                    for kv in range(2):
-                        w_arrived(cc, row_x * groups + g, kv)
-                        w_pass(cc, g, kv).start()
-                    c_add(cc, row_x * groups + g, g == 0)
-                if g > 0:
-                    for kv in range(2):
-                        w_arrived(cc, (1 - row_x) * groups + g - 1, kv)
-                    c_add(cc, (1 - row_x) * groups + g - 1, False)
-            c_finish(cc)
+        w_relay(1, 2, 0)
+        w_own(1, 0, True)
+        w_peer(1, 0)
+        w_own(1, 1)
+        w_relay(1, 2, 1)
+        w_peer(1, 1)
+        w_own(1, 2)
+        w_relay(1, 3, 0)
+        w_relay(1, 3, 1)
+        w_peer(1, 2)
+        for s in range(moved_seq):
+            for o in range(1, n_sp):
+                rs_copy(s, o).start()
+        w_own(1, 3)
+        w_peer(1, 3)
+        c_finish(1)
 
     def gather(s):
         for o in range(1, n_sp):
@@ -906,40 +954,6 @@
             term = jnp.where(sp == j, totals[s], landed[s, j])
             total = term if total is None else total + term
         totals[s] = total
-
-    for s in range(moved_seq):
-        gather(s)
-
-    @pl.when(mid)
-    def _():
-        gather(moved_seq)
-
-    @pl.when(end)
-    def _():
-        for cc in range(chunks):
-            for o in range(n_sp):
-                pltpu.make_async_remote_copy(
-                    stage_c.at[cc, o], landed_c.at[cc, o], c_tx.at[cc, o], c_rx.at[cc, o],
-                    device_id={"sp": o, "tp": mate_tp}, device_id_type=MESH,
-                ).wait_recv()
-            for side in range(2):
-                at = slice(side * half + cc * LANES, side * half + (cc + 1) * LANES)
-                totals[moved_seq, :, at] = landed_c[cc, 2 * side] + landed_c[cc, 2 * side + 1]
-
-    raws = []
-    for s in range(seqs):
-        total = totals[s]
-        kept = total[0:keep].astype(BF16)
-        for h in range(heads):
-            state_out[s, h] = kept[:, h * HD : (h + 1) * HD]
-        raws.append(total[keep : keep + 1] * rows_ref[1:2] + own_term[s : s + 1])
-    raw = jnp.concatenate(raws, axis=0)
-    for h in range(heads):
-        at = slice(h * HD, (h + 1) * HD)
-        head = raw[:, at]
-        centered = head - jnp.mean(head, axis=-1, keepdims=True)
-        spread = jnp.mean(centered * centered, axis=-1, keepdims=True)
-        read_out[:, at] = (centered * lax.rsqrt(spread + 1e-05)).astype(BF16)
 
     for o in range(1, n_tp):
         n_copy(o).wait_send()
@@ -977,8 +991,6 @@
             for g in range(groups):
                 for kv in range(2):
                     w_pass(cc, g, kv).wait_send()
-            for o in range(n_sp):
-                c_copy(cc, o).wait_send()
 
     @pl.loop(0, len(order))
     def _(n):
@@ -995,6 +1007,46 @@
                 to_mate(c, s).wait_send()
 
             to_partner(c, s).wait_send()
+
+    for s in range(moved_seq):
+        gather(s)
+
+    @pl.when(mid)
+    def _():
+        gather(moved_seq)
+
+    @pl.when(end)
+    def _():
+        for cc in range(chunks):
+            for o in range(n_sp):
+                pltpu.make_async_remote_copy(
+                    stage_c.at[cc, o], landed_c.at[cc, o], c_tx.at[cc, o], c_rx.at[cc, o],
+                    device_id={"sp": o, "tp": mate_tp}, device_id_type=MESH,
+                ).wait_recv()
+            for side in range(2):
+                at = slice(side * half + cc * LANES, side * half + (cc + 1) * LANES)
+                totals[moved_seq, :, at] = landed_c[cc, 2 * side] + landed_c[cc, 2 * side + 1]
+
+    raws = []
+    for s in range(seqs):
+        total = totals[s]
+        kept = total[0:keep].astype(BF16)
+        for h in range(heads):
+            state_out[s, h] = kept[:, h * HD : (h + 1) * HD]
+        raws.append(total[keep : keep + 1] * rows_ref[1:2] + own_term[s : s + 1])
+    raw = jnp.concatenate(raws, axis=0)
+    for h in range(heads):
+        at = slice(h * HD, (h + 1) * HD)
+        head = raw[:, at]
+        centered = head - jnp.mean(head, axis=-1, keepdims=True)
+        spread = jnp.mean(centered * centered, axis=-1, keepdims=True)
+        read_out[:, at] = (centered * lax.rsqrt(spread + 1e-05)).astype(BF16)
+
+    @pl.when(mid)
+    def _():
+        for cc in range(chunks):
+            for o in range(n_sp):
+                c_copy(cc, o).wait_send()
 
 
 def solution(mesh):
@@ -1016,7 +1068,7 @@
         anywhere = pl.BlockSpec(memory_space=pl.ANY)
         vmem = pl.BlockSpec(memory_space=pltpu.VMEM)
         dma = pltpu.SemaphoreType.DMA
-        moves = chips == 4 and n_sp == 4 and seqs > 1 and inner % (2 * LANES) == 0
+        moves = chips == 4 and n_sp == 4 and seqs > 1 and inner == 4 * LANES
         tokens_in = [
             pltpu.VMEM((n_tp, pieces, size, feat), BF16),
             pltpu.VMEM((n_tp, seqs, feat), BF16),

time: 131 us -> 107 us (0.82)
  Pallas kernels: 127 us -> 104 us
    pallas_call x1, Pallas kernels: 127 us -> 104 us  [body(): pl.pallas_call(functools.partial(call, n_sp, n_tp, parts), out_shape=(jax...]
where the time goes in v2:
time: 107 us
  Pallas kernels  104 us (97%)
  local copies, waits for them, and re-layouts  2.82 us (3%)
    pallas_call x1, Pallas kernels, body(): pl.pallas_call(functools.partial(call, n_sp, n_tp, parts), out_shape=(jax...  104 us
    unnamed x2, local copies, waits for them, and re-layouts  2.82 us

profile of v2, /device:TPU:0, one launch (start us, length us, event | category | flops | bytes accessed | tf_op | source)
XLA Modules:
  0.0 107.0 jit_solution(295220721840839762)
XLA Ops:
  0.6 103.5 %retention.1 = (bf16[3,8,16,64]{3,2,1,0:T(8,128)(2,1)}, bf16[3,512]{1,0:T(4,128)(2,1)}) custom-call(bf16[3,512,512]{2,1,0:T(8,128)(2,1)} %tokens.1, bf16[3,512]{1,0:T(4,128)(2,1)} %bitcast.1, bf16[4096,512]{1,0:T(8,128)(2,1)} %wq_hbm.1, bf16[4096,512]{1,0:T(8,128)(2,1)} %wk_hbm.1, bf16[4096,512]{1,0:T(8,128)(2,1)} %wv_hbm.1, ...), custom_call_target="tpu_custom_call" | custom-call | tf_op jit(solution)/shard_map/retention/pallas_call | solution.py:1155
  104.1 1.5 %copy.11 = bf16[3,8,16,64]{3,2,1,0:T(8,128)(2,1)} copy(bf16[3,8,16,64]{3,2,1,0:T(8,128)(2,1)} %get-tuple-element.4) | data formatting | bytes 98304
  105.7 1.3 %copy.12 = bf16[3,512]{1,0:T(4,128)(2,1)} copy(bf16[3,512]{1,0:T(4,128)(2,1)} %get-tuple-element.5) | data formatting | bytes 6144

commit v3 on v2

--- a/solution.py
+++ b/solution.py
@@ -401,8 +401,7 @@
     state_out, read_out,
     x, xc, nx, wq, wk, wv, we, acc_k, acc_v, acc_c, cos_ref, sin_ref, fade_ref, rows_ref,
     q_spread, own_term, sums, stage, landed, totals, hint, hint_in, stage_c, landed_c,
-    load_sem, weight_sem, rx, rn, ry, rw, fwd, share, nsend, ysend, yshare, wsend, wxsend,
-    hint_sem, rs_tx, rs_rx, c_tx, c_rx,
+    load_sem, weight_sem, rx, rn, ry, rw, tx, hint_rx, rs_rx, c_rx, ready,
 ):
     seqs, span, feat = tokens.shape
     inner = wk.shape[1]
@@ -415,6 +414,8 @@
     keep = HD // n_sp
     groups = n_tp // 2
     moved_seq = seqs - 1
+    to_mate_tx, to_other_tx, share_tx, n_tx, n_share_tx, y_tx, y_share_tx, w_tx, w_pass_tx = range(9)
+    hint_tx, rs_tx, c_tx = range(9, 12)
     main = list(range(moved_seq * parts))
     moved = list(range(moved_seq * parts, pieces))
     sp = lax.axis_index("sp")
@@ -451,61 +452,56 @@
     ]
 
     barrier = pltpu.get_barrier_semaphore()
-    for o in range(1, n_tp):
-        pl.semaphore_signal(
-            barrier, inc=1, device_id={"tp": lax.rem(tp + o, n_tp)}, device_id_type=MESH
-        )
-    for o in range(1, n_sp):
-        pl.semaphore_signal(
-            barrier, inc=1, device_id={"sp": lax.rem(sp + o, n_sp)}, device_id_type=MESH
-        )
-        pl.semaphore_signal(
-            barrier, inc=1, device_id={"sp": lax.rem(sp + o, n_sp), "tp": mate_tp},
-            device_id_type=MESH,
-        )
-    pl.semaphore_wait(barrier, n_tp - 1 + 2 * (n_sp - 1))
-
-    def x_copy(c, s, sem, target):
-        p = 2 * c + k
+    for target in ({"tp": partner}, {"tp": mate_tp}, {"sp": x_peer}, {"sp": y_peer}):
+        pl.semaphore_signal(barrier, inc=1, device_id=target, device_id_type=MESH)
+
+    @pl.when(mid)
+    def _():
+        pl.semaphore_signal(barrier, inc=1, device_id={"tp": other_tp}, device_id_type=MESH)
+
+    pl.semaphore_wait(barrier, 5 - end_int)
+    for target in ({"sp": x_peer}, {"sp": y_peer}):
+        pl.semaphore_signal(ready.at[0], inc=1, device_id=target, device_id_type=MESH)
+
+    def remote(source, dest, send, recv, target):
         return pltpu.make_async_remote_copy(
-            x.at[p, s], x.at[p, s], sem, rx.at[p, s],
-            device_id={"tp": target}, device_id_type=MESH,
-        )
+            source, dest, send, recv, device_id=target, device_id_type=MESH
+        )
+
+    def sent(ref, kind):
+        remote(ref, ref, tx.at[kind], hint_rx.at[0], {"tp": partner}).wait_send()
+
+    def arrived(ref, sem):
+        remote(ref, ref, tx.at[0], sem, {"tp": partner}).wait_recv()
+
+    def x_copy(c, s, kind, target):
+        here = x.at[2 * c + k, s]
+        return remote(here, here, tx.at[kind], rx.at[2 * c + k, s], {"tp": target})
 
     def to_mate(c, s):
-        return x_copy(c, s, fwd.at[0, c, s], mate_tp)
+        return x_copy(c, s, to_mate_tx, mate_tp)
 
     def to_other(c, s):
-        return x_copy(c, s, fwd.at[1, c, s], other_tp)
+        return x_copy(c, s, to_other_tx, other_tp)
 
     def to_partner(c, s):
-        return x_copy(c, s, share.at[c, s], partner)
+        return x_copy(c, s, share_tx, partner)
 
     def x_arrived(p, s):
-        pltpu.make_async_remote_copy(
-            x.at[p, s], x.at[p, s], share.at[0, 0], rx.at[p, s],
-            device_id={"tp": partner}, device_id_type=MESH,
-        ).wait_recv()
+        arrived(x.at[p, s], rx.at[p, s])
 
     def y_send(c, j):
         p = 2 * c + k
-        return pltpu.make_async_remote_copy(
-            x.at[p, moved[0] + j], xc.at[p, j], ysend.at[c, j], ry.at[p, j],
-            device_id={"sp": y_peer}, device_id_type=MESH,
+        return remote(
+            x.at[p, moved[0] + j], xc.at[p, j], tx.at[y_tx], ry.at[c * parts + j], {"sp": y_peer}
         )
 
     def y_share(c, j):
-        p = 2 * c + k
-        return pltpu.make_async_remote_copy(
-            xc.at[p, j], xc.at[p, j], yshare.at[c, j], ry.at[p, j],
-            device_id={"tp": partner}, device_id_type=MESH,
-        )
-
-    def y_arrived(p, j):
-        pltpu.make_async_remote_copy(
-            xc.at[p, j], xc.at[p, j], yshare.at[0, 0], ry.at[p, j],
-            device_id={"tp": partner}, device_id_type=MESH,
-        ).wait_recv()
+        here = xc.at[2 * c + k, j]
+        late = (c == third).astype(jnp.int32)
+        return remote(
+            here, here, tx.at[y_share_tx], ry.at[chips * parts + late], {"tp": partner}
+        )
 
     def w_rows(p):
         return pl.ds(pl.multiple_of(p * feat, feat), feat)
@@ -513,75 +509,92 @@
     def w_cols(cc):
         return pl.ds(pl.multiple_of(row_y * half + cc * LANES, LANES), LANES)
 
+    def w_place(cc, g, kv):
+        return we.at[cc, w_rows(row_x * groups + g), pl.ds(kv * LANES, LANES)]
+
+    def w_sem(cc, g, kv):
+        return rw.at[g if cc == 0 else groups + 2 * g + kv]
+
+    def w_peer_sem(cc, g):
+        return rw.at[3 * groups + cc * (1 + g)]
+
     def w_send(cc, g, kv):
-        p = row_x * groups + g
-        return pltpu.make_async_remote_copy(
-            (wk, wv)[kv].at[w_rows(p), w_cols(cc)],
-            we.at[cc, w_rows(p), pl.ds(kv * LANES, LANES)],
-            wsend.at[cc, g, kv], rw.at[cc, p, kv],
-            device_id={"tp": mate_tp}, device_id_type=MESH,
-        )
+        mine = (wk, wv)[kv].at[w_rows(row_x * groups + g), w_cols(cc)]
+        return remote(mine, w_place(cc, g, kv), tx.at[w_tx], w_sem(cc, g, kv), {"tp": mate_tp})
 
     def w_pass(cc, g, kv):
-        p = row_x * groups + g
-        where = we.at[cc, w_rows(p), pl.ds(kv * LANES, LANES)]
-        return pltpu.make_async_remote_copy(
-            where, where, wxsend.at[cc, g, kv], rw.at[cc, p, kv],
-            device_id={"sp": x_peer}, device_id_type=MESH,
-        )
-
-    def w_arrived(cc, p, kv):
-        where = we.at[cc, w_rows(p), pl.ds(kv * LANES, LANES)]
-        pltpu.make_async_remote_copy(
-            where, where, wxsend.at[cc, 0, kv], rw.at[cc, p, kv],
-            device_id={"sp": x_peer}, device_id_type=MESH,
-        ).wait_recv()
-
-    def n_copy(o):
-        return pltpu.make_async_remote_copy(
-            nx.at[tp], nx.at[tp], nsend.at[o], rn.at[tp],
-            device_id={"tp": lax.rem(tp + o, n_tp)}, device_id_type=MESH,
-        )
-
-    def n_arrived(o):
-        p = lax.rem(tp + o, n_tp)
-        pltpu.make_async_remote_copy(
-            nx.at[p], nx.at[p], nsend.at[0], rn.at[p],
-            device_id={"tp": p}, device_id_type=MESH,
-        ).wait_recv()
-
-    hint_copy = pltpu.make_async_remote_copy(
-        hint, hint_in, hint_sem.at[0], hint_sem.at[1],
-        device_id={"tp": mate_tp}, device_id_type=MESH,
-    )
+        here = w_place(cc, g, kv)
+        return remote(here, here, tx.at[w_pass_tx], w_peer_sem(cc, g), {"sp": x_peer})
+
+    def n_copy(c, kind, sem, target):
+        here = nx.at[2 * c + k]
+        return remote(here, here, tx.at[kind], sem, {"tp": target})
+
+    def n_to(c, target):
+        n_copy(c, n_tx, rn.at[c], target).start()
+
+    def n_share(c):
+        n_copy(c, n_share_tx, rn.at[chips], partner).start()
+
+    def n_arrived(c):
+        arrived(nx.at[2 * c + k], rn.at[c])
+
+    hint_copy = remote(hint, hint_in, tx.at[hint_tx], hint_rx.at[0], {"tp": mate_tp})
 
     new_load.wait()
-    for o in range(1, n_tp):
-        n_copy(o).start()
-    for j, s in enumerate(moved):
+    n_to(z, mate_tp)
+    n_share(z)
+
+    @pl.when(mid)
+    def _():
+        n_to(z, other_tp)
+
+    for s in moved + main:
         own_loads[s].wait()
 
+    def send_moved(j):
+        s = moved[j]
+
         @pl.when(mid)
-        def _(j=j, s=s):
+        def _():
             to_other(z, s).start()
             y_send(z, j).start()
             to_partner(z, s).start()
 
         @pl.when(end)
-        def _(s=s):
+        def _():
             to_mate(z, s).start()
 
-    for s in main:
-        own_loads[s].wait()
-        to_partner(z, s).start()
-
-        @pl.when(mid)
-        def _(s=s):
-            to_mate(z, s).start()
-            to_other(z, s).start()
+    send_moved(0)
+    to_partner(z, main[0]).start()
+
+    @pl.when(mid)
+    def _():
+        to_mate(z, main[0]).start()
 
     for copy in weight_loads:
         copy.start()
+
+    @pl.when(mid)
+    def _():
+        n_arrived(mate)
+        n_to(mate, other_tp)
+        n_share(mate)
+        n_arrived(other)
+        n_to(other, mate_tp)
+        n_share(other)
+
+    for j in range(1, parts):
+        send_moved(j)
+    for s in main[1:]:
+        to_partner(z, s).start()
+
+    @pl.when(mid)
+    def _():
+        for s in main[1:2]:
+            to_mate(z, s).start()
+        for s in main:
+            to_other(z, s).start()
 
     row = lax.broadcasted_iota(jnp.int32, (span, LANES), 0)
     within = lane_iota((1, LANES)) % HD
@@ -640,6 +653,15 @@
         == lax.broadcasted_iota(jnp.int32, (inner, inner), 1) // HD
     )
     pick = lax.broadcasted_iota(jnp.int32, (HD, inner), 0) == lane_iota((HD, inner)) % HD
+
+    @pl.when(mid)
+    def _():
+        n_arrived(third)
+        n_to(third, mate_tp)
+        n_share(third)
+        for s in main[2:]:
+            to_mate(z, s).start()
+
     own_pieces = end_int * len(main) + (1 - end_int) * pieces
 
     @pl.loop(0, pieces)
@@ -655,8 +677,13 @@
             x_arrived(partner, s)
             add(partner, s, False)
 
-    for o in range(1, n_tp):
-        n_arrived(o)
+    @pl.when(end)
+    def _():
+        for c in (mate, second, third):
+            n_arrived(c)
+            n_share(c)
+
+    arrived(nx.at[pl.ds(0, chips)], rn.at[chips])
 
     def project_new():
         def piece(p, totals):
@@ -704,10 +731,12 @@
 
     def rs_copy(s, o):
         peer = lax.rem(sp + o, n_sp)
-        return pltpu.make_async_remote_copy(
-            stage.at[s, peer], landed.at[s, sp], rs_tx.at[s, peer], rs_rx.at[s, sp],
-            device_id={"sp": peer}, device_id_type=MESH,
-        )
+        return remote(
+            stage.at[s, peer], landed.at[s, sp], tx.at[rs_tx], rs_rx.at[s], {"sp": peer}
+        )
+
+    pl.semaphore_wait(ready.at[0], 2)
+    pl.semaphore_signal(ready.at[1], inc=1, device_id={"sp": x_peer}, device_id_type=MESH)
 
     def outer(weighted, value):
         both = lax.dot_general(
@@ -752,9 +781,9 @@
                     acc_c[side, t] += both
 
     def c_copy(cc, o):
-        return pltpu.make_async_remote_copy(
-            stage_c.at[cc, o], landed_c.at[cc, sp], c_tx.at[cc, o], c_rx.at[cc, sp],
-            device_id={"sp": o, "tp": mate_tp}, device_id_type=MESH,
+        return remote(
+            stage_c.at[cc, o], landed_c.at[cc, sp], tx.at[c_tx], c_rx.at[cc],
+            {"sp": o, "tp": mate_tp},
         )
 
     def c_finish(cc):
@@ -804,19 +833,19 @@
     c_at = len(order) - 3
 
     def w_relay(cc, g, kv):
-        w_arrived(cc, row_x * groups + g, kv)
+        arrived(w_place(cc, g, kv), w_sem(cc, g, kv))
         w_pass(cc, g, kv).start()
 
     def w_own(cc, g, fresh_total=False):
         c_add(cc, row_x * groups + g, fresh_total)
 
     def w_peer(cc, g):
-        for kv in range(2):
-            w_arrived(cc, (1 - row_x) * groups + g, kv)
-        c_add(cc, (1 - row_x) * groups + g, False)
+        p = (1 - row_x) * groups + g
+        arrived(we.at[cc, w_rows(p)], w_peer_sem(cc, g))
+        c_add(cc, p, False)
 
     def y_pass(c, j):
-        y_arrived(2 * c + k, j)
+        arrived(xc.at[2 * c + k, j], ry.at[c * parts + j])
         y_share(c, j).start()
 
     @pl.loop(0, len(order) + 1)
@@ -856,8 +885,10 @@
 
         @pl.when(mid & (n >= first_w) & (n < first_w + groups))
         def _():
+            g = n - first_w
+            arrived(we.at[0, w_rows(row_x * groups + g)], w_sem(0, g, 0))
             for kv in range(2):
-                w_relay(0, n - first_w, kv)
+                w_pass(0, g, kv).start()
 
         @pl.when(mid & (n >= 3) & (n < 3 + parts))
         def _():
@@ -891,12 +922,8 @@
 
         @pl.when(mid & (early == 0))
         def _():
-            for cx in (z, mate, second):
-                for j in range(parts):
-                    y_arrived(2 * cx + 1 - k, j)
-            for g in range(groups):
-                for kv in range(2):
-                    w_arrived(0, (1 - row_x) * groups + g, kv)
+            arrived(xc.at[pl.ds(0, chips - 1)], ry.at[chips * parts])
+            arrived(we.at[0, pl.ds(0, groups * feat)], w_peer_sem(0, 0))
             acc_c[...] = jnp.zeros(acc_c.shape, F32)
 
         @pl.when(mid & (early >= 0) & (early < 6))
@@ -911,8 +938,7 @@
 
         @pl.when(mid & (n == c_at))
         def _():
-            for j in range(parts):
-                y_arrived(2 * third + 1 - k, j)
+            arrived(xc.at[0], ry.at[chips * parts + 1])
 
             @pl.loop(0, 2)
             def _(m):
@@ -921,6 +947,7 @@
             w_relay(1, 0, 0)
 
             hint_copy.wait_recv()
+            pl.semaphore_wait(ready.at[1], 1)
             c_finish(0)
 
     @pl.when(mid)
@@ -943,70 +970,35 @@
         c_finish(1)
 
     def gather(s):
-        for o in range(1, n_sp):
-            src = lax.rem(sp + o, n_sp)
-            pltpu.make_async_remote_copy(
-                stage.at[s, src], landed.at[s, src], rs_tx.at[s, src], rs_rx.at[s, src],
-                device_id={"sp": src}, device_id_type=MESH,
-            ).wait_recv()
+        arrived(landed.at[s, pl.ds(0, n_sp - 1)], rs_rx.at[s])
         total = None
         for j in range(n_sp):
             term = jnp.where(sp == j, totals[s], landed[s, j])
             total = term if total is None else total + term
         totals[s] = total
 
-    for o in range(1, n_tp):
-        n_copy(o).wait_send()
-    for s in main:
-        to_partner(z, s).wait_send()
-        to_mate(z, s).wait_send()
-        for o in range(1, n_sp):
-            if s % parts == 0:
-                rs_copy(s // parts, o).wait_send()
+    sent(nx.at[pl.ds(0, chips)], n_share_tx)
 
     @pl.when(end)
     def _():
-        hint_copy.wait_send()
-        for s in moved:
-            to_mate(z, s).wait_send()
-        for cc in range(chunks):
-            for g in range(groups):
-                for kv in range(2):
-                    w_send(cc, g, kv).wait_send()
+        pl.semaphore_wait(ready.at[1], 1)
+        sent(nx.at[0], n_tx)
+        sent(hint, hint_tx)
+        sent(x.at[0], to_mate_tx)
+        sent(x.at[pl.ds(0, chips), pl.ds(0, len(main))], share_tx)
+        sent(we.at[pl.ds(0, chunks), pl.ds(0, groups * feat)], w_tx)
+        sent(stage.at[pl.ds(0, moved_seq), pl.ds(0, n_sp - 1)], rs_tx)
 
     @pl.when(mid)
     def _():
-        for j, s in enumerate(moved):
-            to_other(z, s).wait_send()
-            to_partner(z, s).wait_send()
-        for s in main:
-            to_other(z, s).wait_send()
-        for cx in range(chips):
-            for j in range(parts):
-                y_send(cx, j).wait_send()
-                y_share(cx, j).wait_send()
-        for o in range(1, n_sp):
-            rs_copy(moved_seq, o).wait_send()
-        for cc in range(chunks):
-            for g in range(groups):
-                for kv in range(2):
-                    w_pass(cc, g, kv).wait_send()
-
-    @pl.loop(0, len(order))
-    def _(n):
-        kind, c, s = decode(n)
-
-        @pl.when(n < steps)
-        def _():
-            @pl.when(mid & (kind == 0))
-            def _():
-                to_other(c, s).wait_send()
-
-            @pl.when(mid & (kind > 0) & (s < moved[0]))
-            def _():
-                to_mate(c, s).wait_send()
-
-            to_partner(c, s).wait_send()
+        sent(nx.at[pl.ds(0, 5)], n_tx)
+        sent(x.at[pl.ds(0, chips - 1), pl.ds(0, len(main))], to_mate_tx)
+        sent(x.at[pl.ds(0, 2)], to_other_tx)
+        sent(x.at[pl.ds(0, chips)], share_tx)
+        sent(xc.at[pl.ds(0, chips)], y_tx)
+        sent(xc.at[pl.ds(0, chips)], y_share_tx)
+        sent(we.at[pl.ds(0, chunks), pl.ds(0, groups * feat)], w_pass_tx)
+        sent(stage.at[:, pl.ds(0, n_sp - 1)], rs_tx)
 
     for s in range(moved_seq):
         gather(s)
@@ -1018,11 +1010,7 @@
     @pl.when(end)
     def _():
         for cc in range(chunks):
-            for o in range(n_sp):
-                pltpu.make_async_remote_copy(
-                    stage_c.at[cc, o], landed_c.at[cc, o], c_tx.at[cc, o], c_rx.at[cc, o],
-                    device_id={"sp": o, "tp": mate_tp}, device_id_type=MESH,
-                ).wait_recv()
+            arrived(landed_c.at[cc], c_rx.at[cc])
             for side in range(2):
                 at = slice(side * half + cc * LANES, side * half + (cc + 1) * LANES)
                 totals[moved_seq, :, at] = landed_c[cc, 2 * side] + landed_c[cc, 2 * side + 1]
@@ -1044,9 +1032,7 @@
 
     @pl.when(mid)
     def _():
-        for cc in range(chunks):
-            for o in range(n_sp):
-                c_copy(cc, o).wait_send()
+        sent(stage_c, c_tx)
 
 
 def solution(mesh):
@@ -1110,21 +1096,14 @@
                     dma((pieces + 1,)),
                     dma((3,)),
                     dma((n_tp, pieces)),
-                    dma((n_tp,)),
-                    dma((n_tp, parts)),
-                    dma((chunks, n_tp, 2)),
-                    dma((2, chips, pieces)),
-                    dma((chips, pieces)),
-                    dma((n_tp,)),
-                    dma((chips, parts)),
-                    dma((chips, parts)),
-                    dma((chunks, groups, 2)),
-                    dma((chunks, groups, 2)),
-                    dma((2,)),
-                    dma((seqs, n_sp)),
-                    dma((seqs, n_sp)),
-                    dma((chunks, n_sp)),
-                    dma((chunks, n_sp)),
+                    dma((chips + 1,)),
+                    dma((chips * parts + 2,)),
+                    dma((4 * groups + 1,)),
+                    dma((12,)),
+                    dma((1,)),
+                    dma((seqs,)),
+                    dma((chunks,)),
+                    pltpu.SemaphoreType.REGULAR((2,)),
                 ]
             )
         else:

time: 107 us -> 102 us (0.953)
  Pallas kernels: 104 us -> 98.7 us
    pallas_call x1, Pallas kernels: 104 us -> 98.7 us  [body(): pl.pallas_call(functools.partial(call, n_sp, n_tp, parts), out_shape=(jax...]
where the time goes in v3:
time: 102 us
  Pallas kernels  98.7 us (97%)
  local copies, waits for them, and re-layouts  2.82 us (3%)
    pallas_call x1, Pallas kernels, body(): pl.pallas_call(functools.partial(call, n_sp, n_tp, parts), out_shape=(jax...  98.7 us
    unnamed x2, local copies, waits for them, and re-layouts  2.82 us

profile of v3, /device:TPU:0, one launch (start us, length us, event | category | flops | bytes accessed | tf_op | source)
XLA Modules:
  0.0 102.1 jit_solution(2549207493952289632)
XLA Ops:
  0.6 98.7 %retention.1 = (bf16[3,8,16,64]{3,2,1,0:T(8,128)(2,1)}, bf16[3,512]{1,0:T(4,128)(2,1)}) custom-call(bf16[3,512,512]{2,1,0:T(8,128)(2,1)} %tokens.1, bf16[3,512]{1,0:T(4,128)(2,1)} %bitcast.1, bf16[4096,512]{1,0:T(8,128)(2,1)} %wq_hbm.1, bf16[4096,512]{1,0:T(8,128)(2,1)} %wk_hbm.1, bf16[4096,512]{1,0:T(8,128)(2,1)} %wv_hbm.1, ...), custom_call_target="tpu_custom_call" | custom-call | tf_op jit(solution)/shard_map/retention/pallas_call | solution.py:1134
  99.3 1.5 %copy.11 = bf16[3,8,16,64]{3,2,1,0:T(8,128)(2,1)} copy(bf16[3,8,16,64]{3,2,1,0:T(8,128)(2,1)} %get-tuple-element.4) | data formatting | bytes 98304
  100.9 1.3 %copy.12 = bf16[3,512]{1,0:T(4,128)(2,1)} copy(bf16[3,512]{1,0:T(4,128)(2,1)} %get-tuple-element.5) | data formatting | bytes 6144

commit v4 on v3

--- a/solution.py
+++ b/solution.py
@@ -391,7 +391,7 @@
     order = [(kind, i) for i in moved for kind in (0, 1)]
     order += [(1, i) for i in main]
     for at in range(max(len(near), len(far))):
-        order += near[at : at + 1] + far[at : at + 1]
+        order += far[at : at + 1] + near[at : at + 1]
     return order
 
 
@@ -509,21 +509,31 @@
     def w_cols(cc):
         return pl.ds(pl.multiple_of(row_y * half + cc * LANES, LANES), LANES)
 
-    def w_place(cc, g, kv):
-        return we.at[cc, w_rows(row_x * groups + g), pl.ds(kv * LANES, LANES)]
-
-    def w_sem(cc, g, kv):
-        return rw.at[g if cc == 0 else groups + 2 * g + kv]
+    def w_part(g, r):
+        if r is None:
+            return w_rows(row_x * groups + g)
+        start = (row_x * groups + g) * feat + r * (feat // 2)
+        return pl.ds(pl.multiple_of(start, feat // 2), feat // 2)
+
+    def w_place(cc, g, kv, r):
+        return we.at[cc, w_part(g, r), pl.ds(kv * LANES, LANES)]
+
+    def w_sem(cc, g, kv, r):
+        if r is None:
+            return rw.at[cc * groups + g]
+        return rw.at[groups + 1 + 4 * (g - 1) + 2 * r + kv]
 
     def w_peer_sem(cc, g):
-        return rw.at[3 * groups + cc * (1 + g)]
-
-    def w_send(cc, g, kv):
-        mine = (wk, wv)[kv].at[w_rows(row_x * groups + g), w_cols(cc)]
-        return remote(mine, w_place(cc, g, kv), tx.at[w_tx], w_sem(cc, g, kv), {"tp": mate_tp})
-
-    def w_pass(cc, g, kv):
-        here = w_place(cc, g, kv)
+        return rw.at[5 * groups - 3 + cc * (1 + g)]
+
+    def w_send(cc, g, kv, r=None):
+        mine = (wk, wv)[kv].at[w_part(g, r), w_cols(cc)]
+        return remote(
+            mine, w_place(cc, g, kv, r), tx.at[w_tx], w_sem(cc, g, kv, r), {"tp": mate_tp}
+        )
+
+    def w_pass(cc, g, kv, r=None):
+        here = w_place(cc, g, kv, r)
         return remote(here, here, tx.at[w_pass_tx], w_peer_sem(cc, g), {"sp": x_peer})
 
     def n_copy(c, kind, sem, target):
@@ -611,9 +621,9 @@
 
     @pl.when(end)
     def _():
-        for g in range(groups):
+        for cc, g in [(0, g) for g in range(groups)] + [(1, 0)]:
             for kv in range(2):
-                w_send(0, g, kv).start()
+                w_send(cc, g, kv).start()
 
     tables(0, sp)
 
@@ -724,10 +734,10 @@
         hint_copy.start()
         for s in main:
             to_mate(z, s).start()
-        for cc in range(1, chunks):
-            for g in range(groups):
+        for g in range(1, groups):
+            for r in range(2):
                 for kv in range(2):
-                    w_send(cc, g, kv).start()
+                    w_send(1, g, kv, r).start()
 
     def rs_copy(s, o):
         peer = lax.rem(sp + o, n_sp)
@@ -737,6 +747,17 @@
 
     pl.semaphore_wait(ready.at[0], 2)
     pl.semaphore_signal(ready.at[1], inc=1, device_id={"sp": x_peer}, device_id_type=MESH)
+
+    def y_half(s):
+        return remote(
+            stage.at[s, pl.ds(2 - 2 * row_y, 2)], landed.at[s, pl.ds(0, 2)],
+            tx.at[rs_tx], rs_rx.at[s], {"sp": y_peer},
+        )
+
+    def x_half(s):
+        return remote(
+            stage.at[s, x_peer], landed.at[s, 2], tx.at[rs_tx], rs_rx.at[seqs + s], {"sp": x_peer}
+        )
 
     def outer(weighted, value):
         both = lax.dot_general(
@@ -769,6 +790,10 @@
             def _():
                 for o in range(1, n_sp):
                     rs_copy(s, o).start()
+
+            @pl.when(mid & (s < moved_seq))
+            def _():
+                y_half(s).start()
 
     def c_add(cc, p, fresh_total):
         where = w_rows(p)
@@ -830,11 +855,17 @@
         return kind, c, s
 
     first_w = 2 * len(moved) + 1
-    c_at = len(order) - 3
-
-    def w_relay(cc, g, kv):
-        arrived(w_place(cc, g, kv), w_sem(cc, g, kv))
-        w_pass(cc, g, kv).start()
+    c_at = len(order) - 4
+    last = len(order) - 1
+
+    def w_pair(cc, g):
+        arrived(we.at[cc, w_part(g, None)], w_sem(cc, g, 0, None))
+        for kv in range(2):
+            w_pass(cc, g, kv).start()
+
+    def w_relay(g, r, kv):
+        arrived(w_place(1, g, kv, r), w_sem(1, g, kv, r))
+        w_pass(1, g, kv, r).start()
 
     def w_own(cc, g, fresh_total=False):
         c_add(cc, row_x * groups + g, fresh_total)
@@ -853,13 +884,13 @@
         kind, c, s = decode(n)
         is_moved = s >= moved[0]
 
-        @pl.when(mid & (n == len(order) - 2))
+        @pl.when(mid & (n == last - 1))
         def _():
             w_relay(1, 0, 1)
 
-        @pl.when(mid & (n == len(order) - 1))
-        def _():
-            w_relay(1, 1, 0)
+        @pl.when(mid & (n == last))
+        def _():
+            w_relay(1, 1, 1)
 
         @pl.when(n < steps)
         def _():
@@ -879,16 +910,25 @@
 
             to_partner(c, s).start()
 
-        @pl.when(mid & (n == len(order) - 1))
-        def _():
-            w_relay(1, 1, 1)
+        @pl.when(mid & (n == last - 2))
+        def _():
+            w_relay(1, 0, 0)
+
+        @pl.when(mid & (n == last - 1))
+        def _():
+            w_relay(1, 1, 0)
+
+        @pl.when(mid & (n == last))
+        def _():
+            w_relay(2, 0, 0)
 
         @pl.when(mid & (n >= first_w) & (n < first_w + groups))
         def _():
-            g = n - first_w
-            arrived(we.at[0, w_rows(row_x * groups + g)], w_sem(0, g, 0))
-            for kv in range(2):
-                w_pass(0, g, kv).start()
+            w_pair(0, n - first_w)
+
+        @pl.when(mid & (n == first_w + groups))
+        def _():
+            w_pair(1, 0)
 
         @pl.when(mid & (n >= 3) & (n < 3 + parts))
         def _():
@@ -907,16 +947,28 @@
         def _():
             add(2 * c + k, s, False)
 
+        @pl.when(mid & (n == last))
+        def _():
+            w_relay(2, 0, 1)
+
         kind_b, c_b, s_b = decode(n - 1)
 
         @pl.when((n >= 1) & (n <= steps))
         def _():
             x_arrived(2 * c_b + 1 - k, s_b)
             add(2 * c_b + 1 - k, s_b, False)
+
+            @pl.when(mid & (n == last + 1))
+            def _():
+                w_relay(2, 1, 1)
 
             @pl.when(kind_b == 2)
             def _():
                 finish(s_b)
+
+        @pl.when(mid & (n == last))
+        def _():
+            w_relay(2, 1, 0)
 
         early = n - (c_at - 5)
 
@@ -944,28 +996,28 @@
             def _(m):
                 c_add(0, 2 * third + m, False)
 
-            w_relay(1, 0, 0)
-
             hint_copy.wait_recv()
             pl.semaphore_wait(ready.at[1], 1)
             c_finish(0)
 
     @pl.when(mid)
     def _():
-        w_relay(1, 2, 0)
         w_own(1, 0, True)
         w_peer(1, 0)
+        w_relay(3, 0, 0)
         w_own(1, 1)
-        w_relay(1, 2, 1)
         w_peer(1, 1)
+        w_relay(3, 0, 1)
         w_own(1, 2)
-        w_relay(1, 3, 0)
-        w_relay(1, 3, 1)
+        w_relay(3, 1, 0)
+        w_relay(3, 1, 1)
         w_peer(1, 2)
+        w_own(1, 3)
         for s in range(moved_seq):
-            for o in range(1, n_sp):
-                rs_copy(s, o).start()
-        w_own(1, 3)
+            arrived(landed.at[s, pl.ds(0, 2)], rs_rx.at[s])
+            for side in range(2):
+                stage[s, 2 * row_y + side] += landed[s, side]
+            x_half(s).start()
         w_peer(1, 3)
         c_finish(1)
 
@@ -1000,15 +1052,17 @@
         sent(we.at[pl.ds(0, chunks), pl.ds(0, groups * feat)], w_pass_tx)
         sent(stage.at[:, pl.ds(0, n_sp - 1)], rs_tx)
 
-    for s in range(moved_seq):
-        gather(s)
-
     @pl.when(mid)
     def _():
+        for s in range(moved_seq):
+            arrived(landed.at[s, 2], rs_rx.at[seqs + s])
+            totals[s] = stage[s, sp] + landed[s, 2]
         gather(moved_seq)
 
     @pl.when(end)
     def _():
+        for s in range(moved_seq):
+            gather(s)
         for cc in range(chunks):
             arrived(landed_c.at[cc], c_rx.at[cc])
             for side in range(2):
@@ -1098,10 +1152,10 @@
                     dma((n_tp, pieces)),
                     dma((chips + 1,)),
                     dma((chips * parts + 2,)),
-                    dma((4 * groups + 1,)),
+                    dma((6 * groups - 2,)),
                     dma((12,)),
                     dma((1,)),
-                    dma((seqs,)),
+                    dma((2 * seqs,)),
                     dma((chunks,)),
                     pltpu.SemaphoreType.REGULAR((2,)),
                 ]

time: 102 us -> 100 us (0.980)
  Pallas kernels: 98.7 us -> 96.3 us
    pallas_call x1, Pallas kernels: 98.7 us -> 96.3 us  [body(): pl.pallas_call(functools.partial(call, n_sp, n_tp, parts), out_shape=(jax...]
where the time goes in v4:
time: 100 us; the launch traced here: 99.8 us
  Pallas kernels  96.3 us (96%)
  local copies, waits for them, and re-layouts  2.82 us (3%)
    pallas_call x1, Pallas kernels, body(): pl.pallas_call(functools.partial(call, n_sp, n_tp, parts), out_shape=(jax...  96.3 us
    unnamed x2, local copies, waits for them, and re-layouts  2.82 us

profile of v4, /device:TPU:0, one launch (start us, length us, event | category | flops | bytes accessed | tf_op | source)
XLA Modules:
  0.0 99.8 jit_solution(11163847009680501896)
XLA Ops:
  0.6 96.3 %retention.1 = (bf16[3,8,16,64]{3,2,1,0:T(8,128)(2,1)}, bf16[3,512]{1,0:T(4,128)(2,1)}) custom-call(bf16[3,512,512]{2,1,0:T(8,128)(2,1)} %tokens.1, bf16[3,512]{1,0:T(4,128)(2,1)} %bitcast.1, bf16[4096,512]{1,0:T(8,128)(2,1)} %wq_hbm.1, bf16[4096,512]{1,0:T(8,128)(2,1)} %wk_hbm.1, bf16[4096,512]{1,0:T(8,128)(2,1)} %wv_hbm.1, ...), custom_call_target="tpu_custom_call" | custom-call | tf_op jit(solution)/shard_map/retention/pallas_call | solution.py:1188
  97.0 1.5 %copy.11 = bf16[3,8,16,64]{3,2,1,0:T(8,128)(2,1)} copy(bf16[3,8,16,64]{3,2,1,0:T(8,128)(2,1)} %get-tuple-element.4) | data formatting | bytes 98304
  98.5 1.3 %copy.12 = bf16[3,512]{1,0:T(4,128)(2,1)} copy(bf16[3,512]{1,0:T(4,128)(2,1)} %get-tuple-element.5) | data formatting | bytes 6144

commit v5 on v4

--- a/solution.py
+++ b/solution.py
@@ -13,6 +13,11 @@
 NEW_ROWS = 8
 F32 = jnp.float32
 BF16 = jnp.bfloat16
+
+
+def inverse_angles():
+    half = HD // 2
+    return np.float32(10000.0) ** (-np.arange(half, dtype=np.float32) / half)
 
 
 def lane_iota(shape):
@@ -395,12 +400,29 @@
     return order
 
 
+def outputs(totals, state_out, read_out):
+    seqs, heads, keep, _ = state_out.shape
+    raws = []
+    for s in range(seqs):
+        kept = totals[s, 0:keep].astype(BF16)
+        for h in range(heads):
+            state_out[s, h] = kept[:, h * HD : (h + 1) * HD]
+        raws.append(totals[s, keep : keep + 1])
+    raw = jnp.concatenate(raws, axis=0)
+    for h in range(heads):
+        at = slice(h * HD, (h + 1) * HD)
+        head = raw[:, at]
+        centered = head - jnp.mean(head, axis=-1, keepdims=True)
+        spread = jnp.mean(centered * centered, axis=-1, keepdims=True)
+        read_out[:, at] = (centered * lax.rsqrt(spread + 1e-05)).astype(BF16)
+
+
 def moved_kernel(
     n_sp, n_tp, parts,
-    tokens, fresh, wq_hbm, wk_hbm, wv_hbm, inverse_ref, decay_ref,
-    state_out, read_out,
+    tokens, fresh, wq_hbm, wk_hbm, wv_hbm, decay_ref,
+    totals,
     x, xc, nx, wq, wk, wv, we, acc_k, acc_v, acc_c, cos_ref, sin_ref, fade_ref, rows_ref,
-    q_spread, own_term, sums, stage, landed, totals, hint, hint_in, stage_c, landed_c,
+    q_spread, own_term, sums, stage, landed, hint, hint_in, stage_c, landed_c,
     load_sem, weight_sem, rx, rn, ry, rw, tx, hint_rx, rs_rx, c_rx, ready,
 ):
     seqs, span, feat = tokens.shape
@@ -609,7 +631,9 @@
     row = lax.broadcasted_iota(jnp.int32, (span, LANES), 0)
     within = lane_iota((1, LANES)) % HD
     first_half = jnp.where(within < HD // 2, -1.0, 1.0).astype(F32)
-    inverse = inverse_ref[...]
+    inverse = jnp.zeros((1, LANES), F32)
+    for j, step in enumerate(inverse_angles()):
+        inverse = jnp.where(within % (HD // 2) == j, float(step), inverse)
 
     def tables(slot, column):
         angles = (column * span + row).astype(F32) * inverse
@@ -1069,20 +1093,9 @@
                 at = slice(side * half + cc * LANES, side * half + (cc + 1) * LANES)
                 totals[moved_seq, :, at] = landed_c[cc, 2 * side] + landed_c[cc, 2 * side + 1]
 
-    raws = []
     for s in range(seqs):
-        total = totals[s]
-        kept = total[0:keep].astype(BF16)
-        for h in range(heads):
-            state_out[s, h] = kept[:, h * HD : (h + 1) * HD]
-        raws.append(total[keep : keep + 1] * rows_ref[1:2] + own_term[s : s + 1])
-    raw = jnp.concatenate(raws, axis=0)
-    for h in range(heads):
-        at = slice(h * HD, (h + 1) * HD)
-        head = raw[:, at]
-        centered = head - jnp.mean(head, axis=-1, keepdims=True)
-        spread = jnp.mean(centered * centered, axis=-1, keepdims=True)
-        read_out[:, at] = (centered * lax.rsqrt(spread + 1e-05)).astype(BF16)
+        read = totals[s, keep : keep + 1]
+        totals[s, keep : keep + 1] = read * rows_ref[1:2] + own_term[s : s + 1]
 
     @pl.when(mid)
     def _():
@@ -1103,8 +1116,7 @@
         parts = max(1, 8 // chips)
         pieces = seqs * parts
         size = span // parts
-        inverse = np.float32(10000.0) ** (-np.arange(half, dtype=np.float32) / half)
-        inverse = jnp.asarray(np.tile(inverse.astype(np.float32), LANES // half)[None])
+        inverse = jnp.asarray(np.tile(inverse_angles(), LANES // half)[None])
         anywhere = pl.BlockSpec(memory_space=pl.ANY)
         vmem = pl.BlockSpec(memory_space=pltpu.VMEM)
         dma = pltpu.SemaphoreType.DMA
@@ -1122,7 +1134,6 @@
             pltpu.VMEM((HD, inner), F32),
             pltpu.VMEM((seqs, n_sp, rows, inner), F32),
             pltpu.VMEM((seqs, n_sp, rows, inner), F32),
-            pltpu.VMEM((seqs, rows, inner), F32),
         ]
         if moves:
             chunks = inner // 2 // LANES
@@ -1173,6 +1184,7 @@
                 ]
                 + ends
                 + [
+                    pltpu.VMEM((seqs, rows, inner), F32),
                     dma((pieces + 1,)),
                     dma((3,)),
                     dma((n_tp, pieces)),
@@ -1185,20 +1197,49 @@
                     dma((seqs, n_sp)),
                 ]
             )
+        out_shape = (
+            jax.ShapeDtypeStruct((seqs, heads, keep, HD), BF16),
+            jax.ShapeDtypeStruct((seqs, inner), BF16),
+        )
+        shared = dict(
+            scratch_shapes=scratch,
+            name="retention",
+        )
+        args = (
+            tokens, new_token.reshape(seqs, feat), query_weight, key_weight, value_weight
+        )
+        args = tuple(pltpu.with_memory_space_constraint(a, pltpu.HBM) for a in args)
+        smem = pl.BlockSpec(memory_space=pltpu.SMEM)
+        limit = (53 if moves else 60) * 1024 * 1024
+        params = pltpu.CompilerParams(
+            collective_id=0, has_side_effects=True, vmem_limit_bytes=limit
+        )
+        call = functools.partial(call, n_sp, n_tp, parts)
+        if not moves:
+            return pl.pallas_call(
+                call,
+                out_shape=out_shape,
+                in_specs=[anywhere] * 5 + [vmem, smem],
+                out_specs=(vmem, vmem),
+                compiler_params=params,
+                **shared,
+            )(*args, inverse, log_decay)
+        sums = pl.pallas_call(
+            call,
+            out_shape=jax.ShapeDtypeStruct((seqs, rows, inner), F32),
+            in_specs=[anywhere] * 5 + [smem],
+            out_specs=vmem,
+            compiler_params=params,
+            **shared,
+        )(*args, pltpu.with_memory_space_constraint(log_decay, pltpu.HBM))
         return pl.pallas_call(
-            functools.partial(call, n_sp, n_tp, parts),
-            out_shape=(
-                jax.ShapeDtypeStruct((seqs, heads, keep, HD), BF16),
-                jax.ShapeDtypeStruct((seqs, inner), BF16),
-            ),
-            in_specs=[anywhere] * 5 + [vmem, pl.BlockSpec(memory_space=pltpu.SMEM)],
+            outputs,
+            out_shape=out_shape,
+            in_specs=[vmem],
             out_specs=(vmem, vmem),
-            scratch_shapes=scratch,
-            compiler_params=pltpu.CompilerParams(
-                collective_id=0, has_side_effects=True, vmem_limit_bytes=60 * 1024 * 1024
-            ),
-            name="retention",
-        )(tokens, new_token.reshape(seqs, feat), query_weight, key_weight, value_weight, inverse, log_decay)
+            compiler_params=pltpu.CompilerParams(vmem_limit_bytes=4 * 1024 * 1024),
+            name="outputs",
+        )(sums)
 
     return jax.shard_map(
         body,

time: 100 us -> 97 us (0.970)
  local copies, waits for them, and re-layouts: 2.82 us -> 0 us
    unnamed x2 -> x0, local copies, waits for them, and re-layouts: 2.82 us -> none
    pallas_call x1 -> x2, Pallas kernels: 96.3 us -> 96.2 us  [the longest x1 95.2 us: body(): pl.pallas_call(call, out_shape=jax.ShapeDtypeStruct((seqs, rows, inner),...]
where the time goes in v5:
time: 97 us; the launch traced here: 96.8 us
  Pallas kernels  96.2 us (99%)
    pallas_call x1, Pallas kernels, body(): pl.pallas_call(call, out_shape=jax.ShapeDtypeStruct((seqs, rows, inner),...  95.2 us

profile of v5, /device:TPU:0, one launch (start us, length us, event | category | flops | bytes accessed | tf_op | source)
XLA Modules:
  0.0 96.8 jit_solution(2021347228548016476)
XLA Ops:
  0.6 95.2 %retention.1.totals = f32[3,24,512]{2,1,0:T(8,128)S(1)} custom-call(bf16[3,512,512]{2,1,0:T(8,128)(2,1)} %tokens.1, bf16[3,512]{1,0:T(4,128)(2,1)} %bitcast.1, bf16[4096,512]{1,0:T(8,128)(2,1)} %wq_hbm.1, bf16[4096,512]{1,0:T(8,128)(2,1)} %wk_hbm.1, bf16[4096,512]{1,0:T(8,128)(2,1)} %wv_hbm.1, f32[8]{0:T(128)} %decay_ref.1), custom_call_target="tpu_custom_call" | custom-call | tf_op jit(solution)/shard_map/retention/pallas_call | solution.py:1227
  95.9 0.9 outputs.1

commit v6 on v5

--- a/solution.py
+++ b/solution.py
@@ -907,6 +907,16 @@
     def _(n):
         kind, c, s = decode(n)
         is_moved = s >= moved[0]
+        kind_b, c_b, s_b = decode(n - 1)
+
+        @pl.when(end & (n >= 1) & (n <= steps))
+        def _():
+            x_arrived(2 * c_b + 1 - k, s_b)
+            add(2 * c_b + 1 - k, s_b, False)
+
+            @pl.when(kind_b == 2)
+            def _():
+                finish(s_b)
 
         @pl.when(mid & (n == last - 1))
         def _():
@@ -975,14 +985,12 @@
         def _():
             w_relay(2, 0, 1)
 
-        kind_b, c_b, s_b = decode(n - 1)
-
-        @pl.when((n >= 1) & (n <= steps))
+        @pl.when(mid & (n >= 1))
         def _():
             x_arrived(2 * c_b + 1 - k, s_b)
             add(2 * c_b + 1 - k, s_b, False)
 
-            @pl.when(mid & (n == last + 1))
+            @pl.when(n == last + 1)
             def _():
                 w_relay(2, 1, 1)
 
@@ -1041,8 +1049,9 @@
             arrived(landed.at[s, pl.ds(0, 2)], rs_rx.at[s])
             for side in range(2):
                 stage[s, 2 * row_y + side] += landed[s, side]
+        w_peer(1, 3)
+        for s in range(moved_seq):
             x_half(s).start()
-        w_peer(1, 3)
         c_finish(1)
 
     def gather(s):

time: 97 us -> 96.1 us (level)
  no operation moved by 1% of the time
where the time goes in v6:
time: 96.1 us; the launch traced here: 95.9 us
  Pallas kernels  95.3 us (99%)
    pallas_call x1, Pallas kernels, body(): pl.pallas_call(call, out_shape=jax.ShapeDtypeStruct((seqs, rows, inner),...  94.3 us

profile of v6, /device:TPU:0, one launch (start us, length us, event | category | flops | bytes accessed | tf_op | source)
XLA Modules:
  0.0 95.9 jit_solution(1253360996551753465)
XLA Ops:
  0.6 94.3 %retention.1.totals = f32[3,24,512]{2,1,0:T(8,128)S(1)} custom-call(bf16[3,512,512]{2,1,0:T(8,128)(2,1)} %tokens.1, bf16[3,512]{1,0:T(4,128)(2,1)} %bitcast.1, bf16[4096,512]{1,0:T(8,128)(2,1)} %wq_hbm.1, bf16[4096,512]{1,0:T(8,128)(2,1)} %wk_hbm.1, bf16[4096,512]{1,0:T(8,128)(2,1)} %wv_hbm.1, f32[8]{0:T(128)} %decay_ref.1), custom_call_target="tpu_custom_call" | custom-call | tf_op jit(solution)/shard_map/retention/pallas_call | solution.py:1236
  95.0 0.9 outputs.1

commit v7 on v6

--- a/solution.py
+++ b/solution.py
@@ -400,21 +400,27 @@
     return order
 
 
-def outputs(totals, state_out, read_out):
+def outputs(totals, state_out, read_out, state, read, sem):
     seqs, heads, keep, _ = state_out.shape
     raws = []
     for s in range(seqs):
         kept = totals[s, 0:keep].astype(BF16)
         for h in range(heads):
-            state_out[s, h] = kept[:, h * HD : (h + 1) * HD]
+            state[s, h] = kept[:, h * HD : (h + 1) * HD]
         raws.append(totals[s, keep : keep + 1])
+    state_copy = pltpu.make_async_copy(state, state_out, sem.at[0])
+    state_copy.start()
     raw = jnp.concatenate(raws, axis=0)
     for h in range(heads):
         at = slice(h * HD, (h + 1) * HD)
         head = raw[:, at]
         centered = head - jnp.mean(head, axis=-1, keepdims=True)
         spread = jnp.mean(centered * centered, axis=-1, keepdims=True)
-        read_out[:, at] = (centered * lax.rsqrt(spread + 1e-05)).astype(BF16)
+        read[:, at] = (centered * lax.rsqrt(spread + 1e-05)).astype(BF16)
+    read_copy = pltpu.make_async_copy(read, read_out, sem.at[1])
+    read_copy.start()
+    state_copy.wait()
+    read_copy.wait()
 
 
 def moved_kernel(
@@ -429,15 +435,15 @@
     inner = wk.shape[1]
     heads = inner // HD
     half = inner // 2
-    chunks = half // LANES
     chips = n_tp // 2
     pieces = seqs * parts
     size = span // parts
     keep = HD // n_sp
-    groups = n_tp // 2
+    units = n_tp
+    early = n_tp - 3
     moved_seq = seqs - 1
-    to_mate_tx, to_other_tx, share_tx, n_tx, n_share_tx, y_tx, y_share_tx, w_tx, w_pass_tx = range(9)
-    hint_tx, rs_tx, c_tx = range(9, 12)
+    to_mate_tx, to_other_tx, share_tx, n_tx, n_share_tx, token_tx, token_share_tx, w_tx = range(8)
+    hint_tx, rs_tx, c_tx = range(8, 11)
     main = list(range(moved_seq * parts))
     moved = list(range(moved_seq * parts, pieces))
     sp = lax.axis_index("sp")
@@ -446,6 +452,7 @@
     row_y, row_x = sp // 2, sp % 2
     x_peer = sp + 1 - 2 * row_x
     y_peer = sp + 2 - 4 * row_y
+    columns = (sp, x_peer, y_peer, x_peer + y_peer - sp)
     MESH = pl.DeviceIdType.MESH
     end_int = (z == 0).astype(jnp.int32) + (z == chips - 1).astype(jnp.int32)
     end = end_int > 0
@@ -512,51 +519,42 @@
     def x_arrived(p, s):
         arrived(x.at[p, s], rx.at[p, s])
 
-    def y_send(c, j):
+    def token_send(c, j):
+        here = x.at[2 * c + k, moved[0] + j]
+        for slot, target in ((0, x_peer), (1, y_peer)):
+            remote(
+                here, xc.at[slot, 2 * c + k, j], tx.at[token_tx],
+                ry.at[(slot * chips + c) * parts + j], {"sp": target},
+            ).start()
+
+    def token_pass(slot, c, j):
         p = 2 * c + k
-        return remote(
-            x.at[p, moved[0] + j], xc.at[p, j], tx.at[y_tx], ry.at[c * parts + j], {"sp": y_peer}
-        )
-
-    def y_share(c, j):
-        here = xc.at[2 * c + k, j]
-        late = (c == third).astype(jnp.int32)
-        return remote(
-            here, here, tx.at[y_share_tx], ry.at[chips * parts + late], {"tp": partner}
-        )
+        here = xc.at[slot, p, j]
+        arrived(here, ry.at[(slot * chips + c) * parts + j])
+        if slot < 2 and slot == j % 2:
+            remote(
+                here, xc.at[2, p, j], tx.at[token_tx],
+                ry.at[(2 * chips + c) * parts + j], {"sp": y_peer if slot == 0 else x_peer},
+            ).start()
+        remote(
+            here, here, tx.at[token_share_tx], ry.at[3 * chips * parts + c], {"tp": partner}
+        ).start()
 
     def w_rows(p):
         return pl.ds(pl.multiple_of(p * feat, feat), feat)
 
-    def w_cols(cc):
-        return pl.ds(pl.multiple_of(row_y * half + cc * LANES, LANES), LANES)
-
-    def w_part(g, r):
-        if r is None:
-            return w_rows(row_x * groups + g)
-        start = (row_x * groups + g) * feat + r * (feat // 2)
-        return pl.ds(pl.multiple_of(start, feat // 2), feat // 2)
-
-    def w_place(cc, g, kv, r):
-        return we.at[cc, w_part(g, r), pl.ds(kv * LANES, LANES)]
-
-    def w_sem(cc, g, kv, r):
-        if r is None:
-            return rw.at[cc * groups + g]
-        return rw.at[groups + 1 + 4 * (g - 1) + 2 * r + kv]
-
-    def w_peer_sem(cc, g):
-        return rw.at[5 * groups - 3 + cc * (1 + g)]
-
-    def w_send(cc, g, kv, r=None):
-        mine = (wk, wv)[kv].at[w_part(g, r), w_cols(cc)]
+    def w_cols():
+        return pl.ds(pl.multiple_of(row_y * half + row_x * LANES, LANES), LANES)
+
+    def w_sem(u, kv):
+        return rw.at[u + (kv if u == units - 1 else 0)]
+
+    def w_send(u, kv):
+        rows = w_rows(2 * (mate, z, second, third)[u // 2] + u % 2)
         return remote(
-            mine, w_place(cc, g, kv, r), tx.at[w_tx], w_sem(cc, g, kv, r), {"tp": mate_tp}
-        )
-
-    def w_pass(cc, g, kv, r=None):
-        here = w_place(cc, g, kv, r)
-        return remote(here, here, tx.at[w_pass_tx], w_peer_sem(cc, g), {"sp": x_peer})
+            (wk, wv)[kv].at[rows, w_cols()], we.at[rows, pl.ds(kv * LANES, LANES)],
+            tx.at[w_tx], w_sem(u, kv), {"tp": mate_tp},
+        )
 
     def n_copy(c, kind, sem, target):
         here = nx.at[2 * c + k]
@@ -590,7 +588,7 @@
         @pl.when(mid)
         def _():
             to_other(z, s).start()
-            y_send(z, j).start()
+            token_send(z, j)
             to_partner(z, s).start()
 
         @pl.when(end)
@@ -645,15 +643,16 @@
 
     @pl.when(end)
     def _():
-        for cc, g in [(0, g) for g in range(groups)] + [(1, 0)]:
+        for u in range(early):
             for kv in range(2):
-                w_send(cc, g, kv).start()
+                w_send(u, kv).start()
 
     tables(0, sp)
 
     @pl.when(mid)
     def _():
-        tables(1, y_peer)
+        for slot in range(1, len(columns)):
+            tables(slot, columns[slot])
 
     new_angles = jnp.full((NEW_ROWS, LANES), n_sp * span, F32) * inverse
     new_cos = jnp.cos(new_angles)
@@ -758,10 +757,9 @@
         hint_copy.start()
         for s in main:
             to_mate(z, s).start()
-        for g in range(1, groups):
-            for r in range(2):
-                for kv in range(2):
-                    w_send(1, g, kv, r).start()
+        for u in range(early, units):
+            for kv in range(2):
+                w_send(u, kv).start()
 
     def rs_copy(s, o):
         peer = lax.rem(sp + o, n_sp)
@@ -819,37 +817,50 @@
             def _():
                 y_half(s).start()
 
-    def c_add(cc, p, fresh_total):
-        where = w_rows(p)
+    def c_add(u, cx, at, halves):
+        p = 2 * cx + u % 2
+        for kv in halves:
+            arrived(we.at[w_rows(p), at], w_sem(u, kv))
         for t in range(parts):
-            for side, block in ((0, x[p, moved[0] + t]), (1, xc[p, t])):
-                both = jnp.dot(block, we[cc, where, :], preferred_element_type=F32)
-                if fresh_total:
-                    acc_c[side, t] = both
+            for slot in range(len(columns)):
+                block = x[p, moved[0] + t] if slot == 0 else xc[slot - 1, p, t]
+                both = jnp.dot(block, we[w_rows(p), at], preferred_element_type=F32)
+                if u == 0:
+                    acc_c[slot, t, :, at] = both
                 else:
-                    acc_c[side, t] += both
-
-    def c_copy(cc, o):
+                    acc_c[slot, t, :, at] += both
+
+    def unit(u):
+        c_add(u, (z, mate, second, third)[u // 2], slice(0, 2 * LANES), (0,))
+
+    def c_copy(o):
         return remote(
-            stage_c.at[cc, o], landed_c.at[cc, sp], tx.at[c_tx], c_rx.at[cc],
-            {"sp": o, "tp": mate_tp},
-        )
-
-    def c_finish(cc):
-        pair_rate = hint_in[1:2, w_cols(cc)]
-        query = hint_in[0:1, w_cols(cc)]
+            stage_c.at[o], landed_c.at[sp], tx.at[c_tx], c_rx.at[0], {"sp": o, "tp": mate_tp}
+        )
+
+    def key_rows(slot, t):
+        return pl.ds((slot * parts + t) * size, size)
+
+    def c_keys():
+        pair_rate = hint_in[1:2, w_cols()]
+        for t in range(parts):
+            at = slice(t * size, (t + 1) * size)
+            fade = jnp.exp(to_end[at] * pair_rate)
+            for slot in range(len(columns)):
+                key = (
+                    rotated(acc_c[slot, t, :, :LANES], cos_ref[slot, at], sin_ref[slot, at])
+                    * HD**-0.5
+                ).astype(BF16)
+                wq[key_rows(slot, t), 0:LANES] = (key.astype(F32) * fade).astype(BF16)
+
+    def c_states():
+        pair_rate = hint_in[1:2, w_cols()]
+        query = hint_in[0:1, w_cols()]
         total = jnp.zeros((HD, LANES), F32)
-        for side, column in ((0, sp), (1, y_peer)):
+        for slot, column in enumerate(columns):
             state = jnp.zeros((HD, LANES), F32)
             for t in range(parts):
-                at = slice(t * size, (t + 1) * size)
-                key = (
-                    rotated(acc_c[side, t, :, :LANES], cos_ref[side, at], sin_ref[side, at])
-                    * HD**-0.5
-                ).astype(BF16)
-                fade = jnp.exp(to_end[at] * pair_rate)
-                weighted = (key.astype(F32) * fade).astype(BF16)
-                state = state + outer(weighted, acc_c[side, t, :, LANES:].astype(BF16))
+                state = state + outer(wq[key_rows(slot, t), 0:LANES], acc_c[slot, t, :, LANES:].astype(BF16))
             total = total + state * jnp.exp(
                 pair_rate * (span * (n_sp - 1 - column)).astype(F32)
             )
@@ -860,10 +871,10 @@
         )
         read = jnp.sum(total * spread, axis=0, keepdims=True)
         for o in range(n_sp):
-            stage_c[cc, o, 0:keep] = total[o * keep : (o + 1) * keep]
-            stage_c[cc, o, keep : keep + 1] = read
+            stage_c[o, 0:keep] = total[o * keep : (o + 1) * keep]
+            stage_c[o, keep : keep + 1] = read
         for o in range(n_sp):
-            c_copy(cc, o).start()
+            c_copy(o).start()
 
     order = middle_order(main, moved)
     steps = end_int * (len(main) * (chips - 1)) + (1 - end_int) * len(order)
@@ -878,30 +889,25 @@
         )
         return kind, c, s
 
-    first_w = 2 * len(moved) + 1
-    c_at = len(order) - 4
     last = len(order) - 1
-
-    def w_pair(cc, g):
-        arrived(we.at[cc, w_part(g, None)], w_sem(cc, g, 0, None))
-        for kv in range(2):
-            w_pass(cc, g, kv).start()
-
-    def w_relay(g, r, kv):
-        arrived(w_place(1, g, kv, r), w_sem(1, g, kv, r))
-        w_pass(1, g, kv, r).start()
-
-    def w_own(cc, g, fresh_total=False):
-        c_add(cc, row_x * groups + g, fresh_total)
-
-    def w_peer(cc, g):
-        p = (1 - row_x) * groups + g
-        arrived(we.at[cc, w_rows(p)], w_peer_sem(cc, g))
-        c_add(cc, p, False)
-
-    def y_pass(c, j):
-        arrived(xc.at[2 * c + k, j], ry.at[c * parts + j])
-        y_share(c, j).start()
+    passes = (
+        (0, ((0, 0, 0), (1, 0, 0))),
+        (1, ((0, 0, 1), (1, 0, 1))),
+        (5, ((0, 1, 0), (1, 1, 0))),
+        (7, ((2, 0, 0), (2, 0, 1), (0, 2, 0), (1, 2, 0))),
+        (8, ((0, 1, 1), (1, 1, 1))),
+        (9, ((0, 2, 1), (1, 2, 1))),
+        (13, ((2, 1, 0), (2, 1, 1))),
+        (15, ((2, 2, 0), (2, 2, 1), (0, 3, 0), (1, 3, 0))),
+        (17, ((0, 3, 1), (1, 3, 1))),
+    )
+    adds = ((8, 0), (9, 1), (14, 2), (15, 3), (16, 4))
+
+    def chip(kind):
+        return (z, mate, second, third)[kind]
+
+    def shared(kind):
+        arrived(xc.at[0, pl.ds(0, 3)], ry.at[3 * chips * parts + chip(kind)])
 
     @pl.loop(0, len(order) + 1)
     def _(n):
@@ -918,14 +924,6 @@
             def _():
                 finish(s_b)
 
-        @pl.when(mid & (n == last - 1))
-        def _():
-            w_relay(1, 0, 1)
-
-        @pl.when(mid & (n == last))
-        def _():
-            w_relay(1, 1, 1)
-
         @pl.when(n < steps)
         def _():
             x_arrived(2 * c + k, s)
@@ -940,119 +938,56 @@
 
             @pl.when(mid & is_moved)
             def _():
-                y_send(c, s - moved[0]).start()
+                token_send(c, s - moved[0])
 
             to_partner(c, s).start()
 
-        @pl.when(mid & (n == last - 2))
-        def _():
-            w_relay(1, 0, 0)
-
-        @pl.when(mid & (n == last - 1))
-        def _():
-            w_relay(1, 1, 0)
-
-        @pl.when(mid & (n == last))
-        def _():
-            w_relay(2, 0, 0)
-
-        @pl.when(mid & (n >= first_w) & (n < first_w + groups))
-        def _():
-            w_pair(0, n - first_w)
-
-        @pl.when(mid & (n == first_w + groups))
-        def _():
-            w_pair(1, 0)
-
-        @pl.when(mid & (n >= 3) & (n < 3 + parts))
-        def _():
-            y_pass(z, n - 3)
-
-        @pl.when(mid & (n >= 6) & (n < 6 + 2 * parts))
-        def _():
-            m = n - 6
-            y_pass((m % 2) * second + (1 - m % 2) * mate, m // 2)
-
-        @pl.when(mid & (n >= c_at - parts) & (n < c_at))
-        def _():
-            y_pass(third, n - (c_at - parts))
+        for step, events in passes:
+
+            @pl.when(mid & (n == step))
+            def _(events=events):
+                for slot, kind, j in events:
+                    token_pass(slot, chip(kind), j)
 
         @pl.when(n < steps)
         def _():
             add(2 * c + k, s, False)
-
-        @pl.when(mid & (n == last))
-        def _():
-            w_relay(2, 0, 1)
 
         @pl.when(mid & (n >= 1))
         def _():
             x_arrived(2 * c_b + 1 - k, s_b)
             add(2 * c_b + 1 - k, s_b, False)
-
-            @pl.when(n == last + 1)
-            def _():
-                w_relay(2, 1, 1)
 
             @pl.when(kind_b == 2)
             def _():
                 finish(s_b)
 
-        @pl.when(mid & (n == last))
-        def _():
-            w_relay(2, 1, 0)
-
-        early = n - (c_at - 5)
-
-        @pl.when(mid & (early == 0))
-        def _():
-            arrived(xc.at[pl.ds(0, chips - 1)], ry.at[chips * parts])
-            arrived(we.at[0, pl.ds(0, groups * feat)], w_peer_sem(0, 0))
-            acc_c[...] = jnp.zeros(acc_c.shape, F32)
-
-        @pl.when(mid & (early >= 0) & (early < 6))
-        def _():
-            turn = early // 2
-            cx = (
-                (turn == 0).astype(jnp.int32) * z
-                + (turn == 1).astype(jnp.int32) * mate
-                + (turn == 2).astype(jnp.int32) * second
-            )
-            c_add(0, 2 * cx + early % 2, False)
-
-        @pl.when(mid & (n == c_at))
-        def _():
-            arrived(xc.at[0], ry.at[chips * parts + 1])
-
-            @pl.loop(0, 2)
-            def _(m):
-                c_add(0, 2 * third + m, False)
-
-            hint_copy.wait_recv()
-            pl.semaphore_wait(ready.at[1], 1)
-            c_finish(0)
+        for step, u in adds:
+
+            @pl.when(mid & (n == step))
+            def _(u=u):
+                if u % 2 == 0:
+                    shared(u // 2)
+                unit(u)
 
     @pl.when(mid)
     def _():
-        w_own(1, 0, True)
-        w_peer(1, 0)
-        w_relay(3, 0, 0)
-        w_own(1, 1)
-        w_peer(1, 1)
-        w_relay(3, 0, 1)
-        w_own(1, 2)
-        w_relay(3, 1, 0)
-        w_relay(3, 1, 1)
-        w_peer(1, 2)
-        w_own(1, 3)
+        hint_copy.wait_recv()
+        pl.semaphore_wait(ready.at[1], 1)
+        unit(early)
+        for j in range(parts):
+            token_pass(2, third, j)
+        shared(3)
+        unit(units - 2)
         for s in range(moved_seq):
             arrived(landed.at[s, pl.ds(0, 2)], rs_rx.at[s])
             for side in range(2):
                 stage[s, 2 * row_y + side] += landed[s, side]
-        w_peer(1, 3)
-        for s in range(moved_seq):
             x_half(s).start()
-        c_finish(1)
+        c_add(units - 1, third, slice(0, LANES), (0,))
+        c_keys()
+        c_add(units - 1, third, slice(LANES, 2 * LANES), (1,))
+        c_states()
 
     def gather(s):
         arrived(landed.at[s, pl.ds(0, n_sp - 1)], rs_rx.at[s])
@@ -1071,7 +1006,7 @@
         sent(hint, hint_tx)
         sent(x.at[0], to_mate_tx)
         sent(x.at[pl.ds(0, chips), pl.ds(0, len(main))], share_tx)
-        sent(we.at[pl.ds(0, chunks), pl.ds(0, groups * feat)], w_tx)
+        sent(we, w_tx)
         sent(stage.at[pl.ds(0, moved_seq), pl.ds(0, n_sp - 1)], rs_tx)
 
     @pl.when(mid)
@@ -1080,9 +1015,8 @@
         sent(x.at[pl.ds(0, chips - 1), pl.ds(0, len(main))], to_mate_tx)
         sent(x.at[pl.ds(0, 2)], to_other_tx)
         sent(x.at[pl.ds(0, chips)], share_tx)
-        sent(xc.at[pl.ds(0, chips)], y_tx)
-        sent(xc.at[pl.ds(0, chips)], y_share_tx)
-        sent(we.at[pl.ds(0, chunks), pl.ds(0, groups * feat)], w_pass_tx)
+        sent(xc.at[:, pl.ds(0, chips)], token_tx)
+        sent(xc.at[:, pl.ds(0, chips)], token_share_tx)
         sent(stage.at[:, pl.ds(0, n_sp - 1)], rs_tx)
 
     @pl.when(mid)
@@ -1096,11 +1030,10 @@
     def _():
         for s in range(moved_seq):
             gather(s)
-        for cc in range(chunks):
-            arrived(landed_c.at[cc], c_rx.at[cc])
-            for side in range(2):
-                at = slice(side * half + cc * LANES, side * half + (cc + 1) * LANES)
-                totals[moved_seq, :, at] = landed_c[cc, 2 * side] + landed_c[cc, 2 * side + 1]
+        arrived(landed_c, c_rx.at[0])
+        for o in range(n_sp):
+            start = (o // 2) * half + (o % 2) * LANES
+            totals[moved_seq, :, start : start + LANES] = landed_c[o]
 
     for s in range(seqs):
         read = totals[s, keep : keep + 1]
@@ -1145,38 +1078,36 @@
             pltpu.VMEM((seqs, n_sp, rows, inner), F32),
         ]
         if moves:
-            chunks = inner // 2 // LANES
-            groups = n_tp // 2
             call = moved_kernel
             scratch = (
                 tokens_in[:1]
-                + [pltpu.VMEM((n_tp, parts, size, feat), BF16)]
+                + [pltpu.VMEM((3, n_tp, parts, size, feat), BF16)]
                 + tokens_in[1:]
                 + weights_in
-                + [pltpu.VMEM((chunks, width, 2 * LANES), BF16)]
+                + [pltpu.VMEM((width, 2 * LANES), BF16)]
                 + totals
                 + [
-                    pltpu.VMEM((2, parts, size, 2 * LANES), F32),
-                    pltpu.VMEM((2, span, LANES), F32),
-                    pltpu.VMEM((2, span, LANES), F32),
+                    pltpu.VMEM((n_sp, parts, size, 2 * LANES), F32),
+                    pltpu.VMEM((n_sp, span, LANES), F32),
+                    pltpu.VMEM((n_sp, span, LANES), F32),
                     pltpu.VMEM((span, inner), F32),
                 ]
                 + ends
                 + [
                     pltpu.VMEM((8, inner), F32),
                     pltpu.VMEM((8, inner), F32),
-                    pltpu.VMEM((chunks, n_sp, rows, LANES), F32),
-                    pltpu.VMEM((chunks, n_sp, rows, LANES), F32),
+                    pltpu.VMEM((n_sp, rows, LANES), F32),
+                    pltpu.VMEM((n_sp, rows, LANES), F32),
                     dma((pieces + 1,)),
                     dma((3,)),
                     dma((n_tp, pieces)),
                     dma((chips + 1,)),
-                    dma((chips * parts + 2,)),
-                    dma((6 * groups - 2,)),
-                    dma((12,)),
+                    dma((3 * chips * parts + chips,)),
+                    dma((n_tp + 1,)),
+                    dma((11,)),
                     dma((1,)),
                     dma((2 * seqs,)),
-                    dma((chunks,)),
+                    dma((1,)),
                     pltpu.SemaphoreType.REGULAR((2,)),
                 ]
             )
@@ -1219,7 +1150,7 @@
         )
         args = tuple(pltpu.with_memory_space_constraint(a, pltpu.HBM) for a in args)
         smem = pl.BlockSpec(memory_space=pltpu.SMEM)
-        limit = (53 if moves else 60) * 1024 * 1024
+        limit = (215 if moves else 240) * 256 * 1024
         params = pltpu.CompilerParams(
             collective_id=0, has_side_effects=True, vmem_limit_bytes=limit
         )
@@ -1245,7 +1176,8 @@
             outputs,
             out_shape=out_shape,
             in_specs=[vmem],
-            out_specs=(vmem, vmem),
+            out_specs=(anywhere, anywhere),
+            scratch_shapes=[pltpu.VMEM(out.shape, BF16) for out in out_shape] + [dma((2,))],
             compiler_params=pltpu.CompilerParams(vmem_limit_bytes=4 * 1024 * 1024),
             name="outputs",
         )(sums)

time: 96.1 us -> 92.8 us (0.966)
  Pallas kernels: 95.3 us -> 91.9 us
    pallas_call x1, Pallas kernels: 94.3 us -> 90.9 us  [body(): pl.pallas_call(call, out_shape=jax.ShapeDtypeStruct((seqs, rows, inner),...]
where the time goes in v7:
time: 92.8 us; the launch traced here: 92.7 us
  Pallas kernels  91.9 us (99%)
    pallas_call x1, Pallas kernels, body(): pl.pallas_call(call, out_shape=jax.ShapeDtypeStruct((seqs, rows, inner),...  90.9 us

profile of v7, /device:TPU:0, one launch (start us, length us, event | category | flops | bytes accessed | tf_op | source)
XLA Modules:
  0.0 92.7 jit_solution(2584928617993774710)
XLA Ops:
  0.6 90.9 %retention.1.totals = f32[3,24,512]{2,1,0:T(8,128)S(1)} custom-call(bf16[3,512,512]{2,1,0:T(8,128)(2,1)} %tokens.1, bf16[3,512]{1,0:T(4,128)(2,1)} %bitcast.1, bf16[4096,512]{1,0:T(8,128)(2,1)} %wq_hbm.1, bf16[4096,512]{1,0:T(8,128)(2,1)} %wk_hbm.1, bf16[4096,512]{1,0:T(8,128)(2,1)} %wv_hbm.1, f32[8]{0:T(128)} %decay_ref.1), custom_call_target="tpu_custom_call" | custom-call | tf_op jit(solution)/shard_map/retention/pallas_call | solution.py:1167
  91.6 0.9 %outputs.1 = (bf16[3,8,16,64]{3,2,1,0:T(8,128)(2,1)}, bf16[3,512]{1,0:T(4,128)(2,1)}) custom-call(f32[3,24,512]{2,1,0:T(8,128)S(1)} %retention.1.totals), custom_call_target="tpu_custom_call" | custom-call | tf_op jit(solution)/shard_map/outputs/pallas_call | solution.py:1175

commit v8 on v7

--- a/solution.py
+++ b/solution.py
@@ -757,9 +757,12 @@
         hint_copy.start()
         for s in main:
             to_mate(z, s).start()
-        for u in range(early, units):
+        final = units - 1
+        for u in range(early, final - 1):
             for kv in range(2):
                 w_send(u, kv).start()
+        for u, kv in ((final, 0), (final - 1, 0), (final - 1, 1), (final, 1)):
+            w_send(u, kv).start()
 
     def rs_copy(s, o):
         peer = lax.rem(sp + o, n_sp)
@@ -978,14 +981,14 @@
         for j in range(parts):
             token_pass(2, third, j)
         shared(3)
+        c_add(units - 1, third, slice(0, LANES), (0,))
         unit(units - 2)
+        c_keys()
         for s in range(moved_seq):
             arrived(landed.at[s, pl.ds(0, 2)], rs_rx.at[s])
             for side in range(2):
                 stage[s, 2 * row_y + side] += landed[s, side]
             x_half(s).start()
-        c_add(units - 1, third, slice(0, LANES), (0,))
-        c_keys()
         c_add(units - 1, third, slice(LANES, 2 * LANES), (1,))
         c_states()
 

time: 92.8 us -> 92.8 us (level)
  no operation moved by 1% of the time
where the time goes in v8:
time: 92.8 us; the launch traced here: 92.7 us
  Pallas kernels  91.9 us (99%)
    pallas_call x1, Pallas kernels, body(): pl.pallas_call(call, out_shape=jax.ShapeDtypeStruct((seqs, rows, inner),...  90.9 us

profile of v8, /device:TPU:0, one launch (start us, length us, event | category | flops | bytes accessed | tf_op | source)
XLA Modules:
  0.0 92.7 jit_solution(9240946966233435481)
XLA Ops:
  0.6 90.9 %retention.1.totals = f32[3,24,512]{2,1,0:T(8,128)S(1)} custom-call(bf16[3,512,512]{2,1,0:T(8,128)(2,1)} %tokens.1, bf16[3,512]{1,0:T(4,128)(2,1)} %bitcast.1, bf16[4096,512]{1,0:T(8,128)(2,1)} %wq_hbm.1, bf16[4096,512]{1,0:T(8,128)(2,1)} %wk_hbm.1, bf16[4096,512]{1,0:T(8,128)(2,1)} %wv_hbm.1, f32[8]{0:T(128)} %decay_ref.1), custom_call_target="tpu_custom_call" | custom-call | tf_op jit(solution)/shard_map/retention/pallas_call | solution.py:1170
  91.6 0.9 %outputs.1 = (bf16[3,8,16,64]{3,2,1,0:T(8,128)(2,1)}, bf16[3,512]{1,0:T(4,128)(2,1)}) custom-call(f32[3,24,512]{2,1,0:T(8,128)S(1)} %retention.1.totals), custom_call_target="tpu_custom_call" | custom-call | tf_op jit(solution)/shard_map/outputs/pallas_call | solution.py:1178

commit v9 on v8

--- a/solution.py
+++ b/solution.py
@@ -643,7 +643,7 @@
 
     @pl.when(end)
     def _():
-        for u in range(early):
+        for u in range(2):
             for kv in range(2):
                 w_send(u, kv).start()
 
@@ -758,7 +758,7 @@
         for s in main:
             to_mate(z, s).start()
         final = units - 1
-        for u in range(early, final - 1):
+        for u in range(2, final - 1):
             for kv in range(2):
                 w_send(u, kv).start()
         for u, kv in ((final, 0), (final - 1, 0), (final - 1, 1), (final, 1)):

time: 92.8 us -> 92.8 us (level)
  no operation moved by 1% of the time
where the time goes in v9:
time: 92.8 us; the launch traced here: 92.6 us
  Pallas kernels  91.8 us (99%)
    pallas_call x1, Pallas kernels, body(): pl.pallas_call(call, out_shape=jax.ShapeDtypeStruct((seqs, rows, inner),...  90.9 us

profile of v9, /device:TPU:0, one launch (start us, length us, event | category | flops | bytes accessed | tf_op | source)
XLA Modules:
  0.0 92.6 jit_solution(12878192596993490701)
XLA Ops:
  0.6 90.9 %retention.1.totals = f32[3,24,512]{2,1,0:T(8,128)S(1)} custom-call(bf16[3,512,512]{2,1,0:T(8,128)(2,1)} %tokens.1, bf16[3,512]{1,0:T(4,128)(2,1)} %bitcast.1, bf16[4096,512]{1,0:T(8,128)(2,1)} %wq_hbm.1, bf16[4096,512]{1,0:T(8,128)(2,1)} %wk_hbm.1, bf16[4096,512]{1,0:T(8,128)(2,1)} %wv_hbm.1, f32[8]{0:T(128)} %decay_ref.1), custom_call_target="tpu_custom_call" | custom-call | tf_op jit(solution)/shard_map/retention/pallas_call | solution.py:1170
  91.5 0.9 %outputs.1 = (bf16[3,8,16,64]{3,2,1,0:T(8,128)(2,1)}, bf16[3,512]{1,0:T(4,128)(2,1)}) custom-call(f32[3,24,512]{2,1,0:T(8,128)S(1)} %retention.1.totals), custom_call_target="tpu_custom_call" | custom-call | tf_op jit(solution)/shard_map/outputs/pallas_call | solution.py:1178
